TPU v7x, 1024 devices: a whole 4x8x16 slice. The times are simulated.
1024 devices in a mesh: rep: 16 (over z), fs: 8 (over y), tp: 8 (over x, core).
Axes of the slice: x: 4, y: 8, z: 16, core: 2. Of those that a mesh axis runs over, the one named last changes fastest.
Arguments:
- layer_input: bfloat16 [12288, 2048], P('rep', ('fs', 'tp')), may hold values from -0.56640625 to 0.56640625
- gate_saved: bfloat16 [12288, 5120], P('rep', 'tp'), may hold values from -6 to 6
- up_saved: bfloat16 [12288, 5120], P('rep', 'tp'), may hold values from -6 to 6
- out_grad: bfloat16 [12288, 2048], P('rep'), may hold values from -0.56640625 to 0.56640625
- conv_taps: bfloat16 [3, 5120], P(None, 'tp'), may hold values from -3.5 to 3.5
- w_gate: bfloat16 [2048, 5120], P('fs', 'tp'), may hold values from -0.125 to 0.125
- w_up: bfloat16 [2048, 5120], P('fs', 'tp'), may hold values from -0.125 to 0.125
- w_down: bfloat16 [5120, 2048], P('tp', 'fs'), may hold values from -0.078125 to 0.078125
Outputs:
- input_grad: bfloat16 [12288, 2048], P('rep', ('fs', 'tp'))
- gate_grad: float32 [2048, 5120], P('fs', 'tp')
- up_grad: float32 [2048, 5120], P('fs', 'tp')
- down_grad: float32 [5120, 2048], P('tp', 'fs')
- taps_grad: float32 [3, 5120], P(None, 'tp')
All inputs are finite; a program needn't handle non-finite values.
Results may differ from a plain program's by a relative error of at most 0.018.
Values may be sent and summed in bfloat16 or wider, within the bound.
No kernel may reach another device: no remote copies, remote signals or barrier semaphores. Data moves between devices by JAX's collectives and lax.ppermute only.
A program may use at most 64 MiB of HBM per device.

v0:
```python
import jax
import jax.numpy as jnp
from jax import lax
from jax.sharding import PartitionSpec as P


def copy_for_each(array, axis):
    length = lax.axis_size(axis)
    return lax.all_to_all(
        jnp.broadcast_to(array[None], (length, *array.shape)), axis, 0, 0, tiled=True
    )


def laid_out(parts, dim):
    lengths = list(parts.shape[1:])
    lengths[dim] *= parts.shape[0]
    return jnp.moveaxis(parts, 0, dim).reshape(lengths)


def gather_directly(array, axis, dim):
    parts = copy_for_each(array, axis)
    return laid_out(parts, dim)


def in_blocks(array, dim, length):
    before, after = (array.shape[:dim], array.shape[dim + 1 :])
    return jnp.moveaxis(array.reshape(*before, length, -1, *after), dim, 0)


def summed_on_arrival(array, axis, dim):
    length = lax.axis_size(axis)
    parts = lax.all_to_all(in_blocks(array, dim, length), axis, 0, 0, tiled=True)
    return jnp.sum(parts.astype(jnp.float32), axis=0)


def swish_cells(gate_cols, up_cols, conv_taps, act_grad):
    gate_float = gate_cols.astype(jnp.float32)
    taps_float = conv_taps.astype(jnp.float32)
    up_float = up_cols.astype(jnp.float32)
    row_count = gate_float.shape[0]
    back_one = jnp.pad(gate_float, ((1, 0), (0, 0)))[:row_count]
    back_two = jnp.pad(gate_float, ((2, 0), (0, 0)))[:row_count]
    conv_out = taps_float[0] * back_two + taps_float[1] * back_one + taps_float[2] * gate_float
    gate_sig = jax.nn.sigmoid(conv_out)
    swish_out = conv_out * gate_sig
    activation = (swish_out * up_float).astype(jnp.bfloat16)
    up_part = (act_grad * swish_out).astype(jnp.bfloat16)
    conv_grad = act_grad * up_float * gate_sig * (1.0 + conv_out * (1.0 - gate_sig))
    ahead_one = jnp.pad(conv_grad, ((0, 1), (0, 0)))[1:]
    ahead_two = jnp.pad(conv_grad, ((0, 2), (0, 0)))[2:]
    gate_part = (
        taps_float[0] * ahead_two + taps_float[1] * ahead_one + taps_float[2] * conv_grad
    ).astype(jnp.bfloat16)
    taps_part = jnp.stack(
        [
            jnp.sum(conv_grad * back_two, axis=0),
            jnp.sum(conv_grad * back_one, axis=0),
            jnp.sum(conv_grad * gate_float, axis=0),
        ]
    )
    return (activation, up_part, gate_part, taps_part)


def token_product(left, right):
    return lax.dot_general(
        left, right, (((0,), (0,)), ((), ())), preferred_element_type=jnp.float32
    )


def width_product(left, right):
    return lax.dot_general(
        left, right, (((1,), (1,)), ((), ())), preferred_element_type=jnp.float32
    )


def local(layer_input, gate_saved, up_saved, out_grad, conv_taps, w_gate, w_up, w_down):
    input_block = gather_directly(layer_input, "tp", 1)
    width_rows = w_gate.shape[0]
    grad_block = lax.dynamic_slice_in_dim(
        out_grad, lax.axis_index("fs") * width_rows, width_rows, 1
    )
    act_grad = width_product(out_grad, lax.all_gather(w_down, "fs", axis=1, tiled=True))
    activation, up_part, gate_part, taps_part = swish_cells(
        gate_saved, up_saved, conv_taps, act_grad
    )
    gate_grad, up_grad, down_grad, taps_grad = (
        lax.psum(token_product(input_block, gate_part).astype(jnp.bfloat16), "rep").astype(
            jnp.float32
        ),
        lax.psum(token_product(input_block, up_part).astype(jnp.bfloat16), "rep").astype(
            jnp.float32
        ),
        lax.psum(token_product(activation, grad_block).astype(jnp.bfloat16), "rep").astype(
            jnp.float32
        ),
        lax.psum(taps_part.astype(jnp.bfloat16), "rep").astype(jnp.float32),
    )
    input_terms = width_product(gate_part, w_gate) + width_product(up_part, w_up)
    input_grad = summed_on_arrival(input_terms.astype(jnp.bfloat16), "tp", 1).astype(jnp.bfloat16)
    return (input_grad, gate_grad, up_grad, down_grad, taps_grad)


def solution(mesh):
    placed = (
        P("rep", ("fs", "tp")),
        P("rep", "tp"),
        P("rep", "tp"),
        P("rep", None),
        P(None, "tp"),
        P("fs", "tp"),
        P("fs", "tp"),
        P("tp", "fs"),
    )
    return jax.shard_map(
        local,
        mesh=mesh,
        in_specs=placed,
        out_specs=(
            P("rep", ("fs", "tp")),
            P("fs", "tp"),
            P("fs", "tp"),
            P("tp", "fs"),
            P(None, "tp"),
        ),
        check_vma=False,
    )
```

profile of v0, /device:TPU:6, one launch (start us, length us, event | category | flops | bytes accessed | tf_op | source)
XLA Modules:
  0.0 256.5 jit_solution(15903712912939512005)
XLA Ops:
  7.2 0.0 all-gather.2.cloned.1.call-start
  7.2 0.7 all-gather.2.cloned.1.call-update
  7.9 1.8 broadcast_in_dim.2
  9.7 16.5 %all-to-all-start.1 = ((bf16[8,768,32]{1,2,0:T(8,128)(2,1)}), bf16[8,768,32]{1,2,0:T(8,128)(2,1)S(1)}, u32[]{:S(2)}, u32[]{:S(2)}) async-start(bf16[8,768,32]{1,2,0:T(8,128)(2,1)} %broadcast_in_dim.2), calls=%async_computation.1 | async-start | bytes 786432 | tf_op jit(solution)/shard_map/all_to_all | solution.py:9
  26.2 0.7 convert_element_type.59
  26.9 2.6 %convert_element_type.61 = f32[768,640]{1,0:T(8,128)} convert(bf16[768,640]{1,0:T(8,128)(2,1)} %param.9) | non-fusion elementwise | flops 491520 | bytes 2949120 | tf_op jit(solution)/shard_map/convert_element_type | solution.py:37
  29.5 0.6 slice_reduce_fusion.2
  30.1 47.5 %all-gather.2.cloned.1.call-done = bf16[640,2048]{1,0:T(8,128)(2,1)} async-done(((bf16[640,256]{1,0:T(8,128)(2,1)}), bf16[640,2048]{1,0:T(8,128)(2,1)}) %all-gather.2.cloned.1.call-update) | async-done | bytes 2621456 | tf_op jit(solution)/shard_map/all_gather | solution.py:82
  77.6 10.3 %multiply_reduce_fusion.2 = (bf16[640]{0:T(1024)(128)(2,1)}, bf16[640]{0:T(1024)(128)(2,1)}, bf16[640]{0:T(1024)(128)(2,1)S(1)}, f32[768,640]{1,0:T(8,128)S(1)},...) fusion(f32[768,640]{1,0:T(8,128)} %convert_element_type.61, bf16[768,640]{1,0:T(8,128)(2,1)} %param.9, ...), kind=kOutput, calls=%fused_computation.16 | convolution fusion | flops 2024077440 | bytes 15609088 | tf_op jit(solution)/shard_map/dot_general | solution.py:71
  87.9 1.3 copy-done.2
  89.2 2.3 fusion.3
  91.5 2.5 fusion.10
  94.0 2.4 fusion.11
  96.4 1.6 convolution_convert_fusion
  98.0 1.9 fusion.18
  100.0 1.3 fusion.9
  101.2 5.7 %all-to-all-start = ((bf16[8,768,32]{1,2,0:T(8,128)(2,1)}), bf16[8,768,32]{1,2,0:T(8,128)(2,1)S(1)}, u32[]{:S(2)}, u32[]{:S(2)}) async-start(bf16[8,768,32]{1,2,0:T(8,128)(2,1)} %bitcast.20), calls=%async_computation | async-start | bytes 786432 | tf_op jit(solution)/shard_map/all_to_all | solution.py:32
  107.0 32.0 %psum.31 = bf16[3,640]{1,0:T(4,128)(2,1)S(1)} all-reduce(bf16[3,640]{1,0:T(4,128)(2,1)S(1)} %pad_maximum_fusion), channel_id=1, replica_groups=mesh['rep'=16,'fs'=8,'tp'=8] {'rep'}, use_global_device_ids=true, to_apply=%region_7.8 | all-reduce | flops 1920 | bytes 7680 | tf_op jit(solution)/shard_map/psum | solution.py:96
  139.1 0.6 convert_element_type.74
  139.7 0.7 reduce_sum.39
  140.3 104.4 %all-reduce.7.cloned.1.call-done = (bf16[256,640]{0,1:T(8,128)(2,1)}, bf16[256,640]{0,1:T(8,128)(2,1)}, bf16[640,256]{1,0:T(8,128)(2,1)}) async-done(((bf16[256,640]{0,1:T(8,128)(2,1)}, bf16[256,640]{0,1:T(8,128)(2,1)}, bf16[640,256]{1,0:T(8,128)(2,1)}), (bf16[256,640]{0,1:T(8,128)(2,1)}, bf16[256,640]{0,1:T(8,128)(2,1)}, bf16[640,256]{1,0:T(8,128)(2,1)})) %all-reduce.7.cloned.1.call-update) | async-done | bytes 983056 | tf_op jit(solution)/shard_map/psum | solution.py:87
  244.8 1.9 convert_element_type.73
  246.7 2.0 copy.16
  248.7 1.0 copy.17
  (29 shorter events, 0.1 us)
Async XLA Ops:
  7.2 70.4 %copy-start = (bf16[768,2048]{1,0:T(8,128)(2,1)S(1)}, bf16[768,2048]{1,0:T(8,128)(2,1)}, u32[]{:S(2)}) copy-start(bf16[768,2048]{1,0:T(8,128)(2,1)} %param.11) | copy-start | bytes 9437188
  7.2 70.4 %all-gather.2.cloned.1.call-start = ((), (), s32[]{:S(2)}) async-start(), calls=%async_computation.2 | async-start | bytes 2949120 | tf_op jit(solution)/shard_map/all_gather | solution.py:82
  9.7 81.8 %all-to-all-start.1 = ((bf16[8,768,32]{1,2,0:T(8,128)(2,1)}), bf16[8,768,32]{1,2,0:T(8,128)(2,1)S(1)}, u32[]{:S(2)}, u32[]{:S(2)}) async-start(bf16[8,768,32]{1,2,0:T(8,128)(2,1)} %broadcast_in_dim.2), calls=%async_computation.1 | async-start | bytes 786432 | tf_op jit(solution)/shard_map/all_to_all | solution.py:9
  26.2 218.6 %all-reduce.7.cloned.1.call-start = ((), (), s32[]{:S(2)}) async-start(), calls=%async_computation.3 | async-start | bytes 1966080 | tf_op jit(solution)/shard_map/psum | solution.py:87
  77.6 11.5 %copy-start.6 = (f32[640]{0:T(1024)S(1)}, f32[640]{0:T(1024)}, u32[]{:S(2)}) copy-start(f32[640]{0:T(1024)} %get-tuple-element.19) | copy-start | bytes 7684
  77.6 11.5 %copy-start.7 = (f32[640]{0:T(1024)S(1)}, f32[640]{0:T(1024)}, u32[]{:S(2)}) copy-start(f32[640]{0:T(1024)} %get-tuple-element.20) | copy-start | bytes 7684
  87.9 1.3 copy-start.2
  91.5 4.9 %copy-start.3 = (f32[768,640]{1,0:T(8,128)S(1)}, f32[768,640]{1,0:T(8,128)}, u32[]{:S(2)}) copy-start(f32[768,640]{1,0:T(8,128)} %copy-done.2) | copy-start | bytes 5898244
  91.5 4.9 %copy-start.10 = (bf16[768,640]{1,0:T(8,128)(2,1)S(1)}, bf16[768,640]{1,0:T(8,128)(2,1)}, u32[]{:S(2)}) copy-start(bf16[768,640]{1,0:T(8,128)(2,1)} %param.10) | copy-start | bytes 2949124
  98.0 1.9 copy-start.4
  98.0 1.9 copy-start.1
  99.9 7.0 %copy-start.9 = (bf16[640]{0:T(1024)(128)(2,1)S(1)}, bf16[640]{0:T(1024)(128)(2,1)}, u32[]{:S(2)}) copy-start(bf16[640]{0:T(1024)(128)(2,1)} %get-tuple-element.15) | copy-start | bytes 3844
  100.0 7.0 %copy-start.8 = (bf16[640]{0:T(1024)(128)(2,1)S(1)}, bf16[640]{0:T(1024)(128)(2,1)}, u32[]{:S(2)}) copy-start(bf16[640]{0:T(1024)(128)(2,1)} %get-tuple-element.16) | copy-start | bytes 3844
  101.2 38.5 %all-to-all-start = ((bf16[8,768,32]{1,2,0:T(8,128)(2,1)}), bf16[8,768,32]{1,2,0:T(8,128)(2,1)S(1)}, u32[]{:S(2)}, u32[]{:S(2)}) async-start(bf16[8,768,32]{1,2,0:T(8,128)(2,1)} %bitcast.20), calls=%async_computation | async-start | bytes 786432 | tf_op jit(solution)/shard_map/all_to_all | solution.py:32
  244.8 3.9 %copy-start.5 = (bf16[256,640]{0,1:T(8,128)(2,1)S(1)}, bf16[256,640]{0,1:T(8,128)(2,1)}, u32[]{:S(2)}) copy-start(bf16[256,640]{0,1:T(8,128)(2,1)} %get-tuple-element.22) | copy-start | bytes 983044
Sparse Core Ops, SparseCore 0:
  10.6 66.9 all-gather.1
  98.2 146.5 all-reduce.6
where the time goes:
time: 257 us
  waiting for transfers between devices  153 us (60%)
  blocking collectives  32 us (12%)
  starting transfers between devices  22.3 us (9%)
  matrix products  19.9 us (8%)
  between operations  14.1 us (5%)
  other arithmetic  8.8 us (3%)
  local copies, waits for them, and re-layouts  6.72 us (3%)
    psum x1, waiting for transfers between devices, local(): lax.psum(token_product(input_block, gate_part).astype(jnp.bfloat16), 'rep')  104 us
    all_gather x1, waiting for transfers between devices, local(): lax.all_gather(w_down, 'fs', axis=1, tiled=True)  47.5 us
    psum x1, blocking collectives, local(): lax.psum(taps_part.astype(jnp.bfloat16), 'rep').astype(jnp.float32)  32 us
    all_to_all x1, starting transfers between devices, copy_for_each(): lax.all_to_all(jnp.broadcast_to(array[None], (length, *array.shape)), axi...  16.5 us
    dot_general x3, matrix products, width_product(): lax.dot_general(left, right, (((1,), (1,)), ((), ())), preferred_element_...  13.4 us
    dot_general x3, matrix products, token_product(): lax.dot_general(left, right, (((0,), (0,)), ((), ())), preferred_element_...  6.51 us
    all_to_all x1, starting transfers between devices, summed_on_arrival(): lax.all_to_all(in_blocks(array, dim, length), axis, 0, 0, tiled=True)  5.74 us
  transfers between devices with their start and end apart: 4, of which 2 were waited for; matrix products, arithmetic and copies ran while one was open for 9% of the time, Pallas kernels for 0%

commit v1 on v0

v1 whole, which is shorter than its diff:
```python
import jax
import jax.numpy as jnp
from jax import lax
from jax.experimental import pallas as pl
from jax.experimental.pallas import tpu as pltpu
from jax.sharding import PartitionSpec as P

LANES = 128
ROWS = 8
DOWN_ROWS = 32
TAPS = 3


def product(left, right, dims):
    return lax.dot_general(left, right, (dims, ((), ())), preferred_element_type=jnp.float32)


def moved(values, count):
    tokens = values.shape[0]
    row = lax.broadcasted_iota(jnp.int32, values.shape, 0)
    inside = (row >= count) if count > 0 else (row < tokens + count)
    return jnp.where(inside, pltpu.roll(values, count % tokens, 0), 0.0)


def lanes_of(c):
    return pl.ds(pl.multiple_of(c * LANES, LANES), LANES)


def split_rows(out, values):
    rows = out[0].shape[0]
    for i, ref in enumerate(out):
        ref[...] = values[i * rows : (i + 1) * rows]


def slabs(length, rows, width):
    return [pltpu.VMEM((rows, width), jnp.bfloat16)] * (length // rows)


def whole(array):
    return pl.BlockSpec(array.shape, lambda c, *_: (0,) * len(array.shape))


def conv_kernel(place, gate, up, taps, grad, down, swish_out, slope_out, *refs):
    down_out, act_out = refs[: LANES // DOWN_ROWS], refs[LANES // DOWN_ROWS :]
    share = product(grad[...], down[...], ((1,), (1,))).astype(jnp.bfloat16)
    for i, ref in enumerate(act_out):
        ref[:, lanes_of(pl.program_id(0))] = share[i * ROWS : (i + 1) * ROWS]
    gate_float = gate[...].astype(jnp.float32)
    up_float = up[...].astype(jnp.float32)
    taps_float = taps[...].astype(jnp.float32)
    conv_out = (
        taps_float[0:1] * moved(gate_float, 2)
        + taps_float[1:2] * moved(gate_float, 1)
        + taps_float[2:3] * gate_float
    )
    sig = jax.nn.sigmoid(conv_out)
    swish = conv_out * sig
    swish_out[...] = swish.astype(jnp.bfloat16)
    slope_out[...] = (up_float * sig * (1.0 + conv_out * (1.0 - sig))).astype(jnp.bfloat16)
    activation = (swish * up_float).astype(jnp.bfloat16)
    split_rows(down_out, product(activation, grad[...], ((0,), (0,))).astype(jnp.bfloat16))


def conv_cells(place, gate_saved, up_saved, conv_taps, out_grad, w_down):
    tokens, hidden = gate_saved.shape
    block = w_down.shape[1]
    acts = slabs(tokens, ROWS, hidden)
    columns = pl.BlockSpec((tokens, LANES), lambda c, s: (0, c))
    cells = pltpu.HBM((tokens, hidden), jnp.bfloat16)
    run = LANES // DOWN_ROWS
    down = pltpu.HBM((hidden // run, block), jnp.bfloat16)
    return pl.pallas_call(
        conv_kernel,
        out_shape=[cells, cells] + [down] * run + acts,
        grid_spec=pltpu.PrefetchScalarGridSpec(
            num_scalar_prefetch=1,
            grid=(hidden // LANES,),
            in_specs=[
                columns,
                columns,
                pl.BlockSpec((TAPS, LANES), lambda c, s: (0, c)),
                pl.BlockSpec((tokens, block), lambda c, s: (0, s[0])),
                pl.BlockSpec((LANES, block), lambda c, s: (c, 0)),
            ],
            out_specs=[columns, columns]
            + [pl.BlockSpec((DOWN_ROWS, block), lambda c, s: (c, 0))] * run
            + [whole(a) for a in acts],
        ),
        compiler_params=pltpu.CompilerParams(vmem_limit_bytes=16 << 20),
        name="conv_cells",
    )(place, gate_saved, up_saved, conv_taps, out_grad, w_down)


def taken(refs, counts):
    runs = []
    for count in counts:
        runs.append(refs[:count])
        refs = refs[count:]
    return *runs, refs


def grad_kernel(counts, taps, swish, slope, gate, inputs, w_gate, w_up, *refs):
    acts, downs, (terms_out, taps_out), gate_out, up_out, down_out, (terms,) = taken(refs, counts)
    c = pl.program_id(0)
    for i, down in enumerate(downs):
        for j in range(len(down_out) // len(downs)):

            @pl.when(c == j)
            def copy(ref=down_out[j * len(downs) + i], down=down):
                ref[...] = down[...]

    act_grad = jnp.concatenate([a[:, lanes_of(c)] for a in acts], 0).astype(jnp.float32)
    up_part = (act_grad * swish[...].astype(jnp.float32)).astype(jnp.bfloat16)
    conv_grad = act_grad * slope[...].astype(jnp.float32)
    taps_float = taps[...].astype(jnp.float32)
    ahead_one, ahead_two = moved(conv_grad, -1), moved(conv_grad, -2)
    gate_part = (
        taps_float[0:1] * ahead_two + taps_float[1:2] * ahead_one + taps_float[2:3] * conv_grad
    ).astype(jnp.bfloat16)
    gate_float = gate[...].astype(jnp.float32)
    sums = [
        jnp.sum(ahead * gate_float, axis=0, keepdims=True)
        for ahead in (ahead_two, ahead_one, conv_grad)
    ]
    taps_out[:, lanes_of(c)] = jnp.concatenate(sums, 0).astype(jnp.bfloat16)
    for out, part in ((gate_out, gate_part), (up_out, up_part)):
        grads = product(inputs[...], part, ((1,), (0,))).astype(jnp.bfloat16)
        for i, ref in enumerate(out):
            ref[:, lanes_of(c)] = grads[i * ROWS : (i + 1) * ROWS]
    term = product(w_gate[...], gate_part, ((1,), (1,))) + product(w_up[...], up_part, ((1,), (1,)))

    @pl.when(c == 0)
    def first():
        terms[...] = term

    @pl.when(c > 0)
    def later():
        terms[...] += term

    @pl.when(c == pl.num_programs(0) - 1)
    def last():
        terms_out[...] = terms[...].astype(jnp.bfloat16)


def grad_cells(conv_taps, swish, slope, gate_saved, inputs, w_gate, w_up, acts, downs):
    tokens, hidden = swish.shape
    block = inputs.shape[0]
    columns = pl.BlockSpec((tokens, LANES), lambda c: (0, c))
    weights = pl.BlockSpec((block, LANES), lambda c: (0, c))
    grads = slabs(block, ROWS, hidden)
    kept = slabs(hidden, DOWN_ROWS, block)
    out = [
        pltpu.HBM((block, tokens), jnp.bfloat16),
        pltpu.VMEM((TAPS, hidden), jnp.bfloat16),
    ] + grads * 2 + kept
    counts = [len(acts), len(downs), 2, len(grads), len(grads), len(kept)]
    return pl.pallas_call(
        lambda *refs: grad_kernel(counts, *refs),
        out_shape=out,
        grid=(hidden // LANES,),
        in_specs=[pl.BlockSpec((TAPS, LANES), lambda c: (0, c)), columns, columns, columns]
        + [whole(inputs), weights, weights]
        + [whole(a) for a in acts]
        + [pl.BlockSpec((DOWN_ROWS, block), lambda c: (c, 0))] * len(downs),
        out_specs=[whole(o) for o in out],
        scratch_shapes=[pltpu.VMEM((block, tokens), jnp.float32)],
        compiler_params=pltpu.CompilerParams(vmem_limit_bytes=24 << 20),
        name="grad_cells",
    )(conv_taps, swish, slope, gate_saved, inputs, w_gate, w_up, *acts, *downs)


def widen_kernel(counts, *refs):
    ins, outs = refs[: sum(counts)], refs[sum(counts) :]
    for out, count in zip(outs, counts):
        rows = out.shape[0] // count
        for i, ref in enumerate(ins[:count]):
            out[i * rows : (i + 1) * rows, :] = ref[...].astype(jnp.float32)
        ins = ins[count:]


def widened(groups):
    out = [
        jax.ShapeDtypeStruct((sum(a.shape[0] for a in g), g[0].shape[1]), jnp.float32)
        for g in groups
    ]
    return pl.pallas_call(
        lambda *refs: widen_kernel([len(g) for g in groups], *refs),
        out_shape=out,
        compiler_params=pltpu.CompilerParams(vmem_limit_bytes=16 << 20),
        name="widened",
    )(*[a for g in groups for a in g])


def local(layer_input, gate_saved, up_saved, out_grad, conv_taps, w_gate, w_up, w_down):
    gate_saved, up_saved, out_grad, w_gate, w_up, w_down = [
        pltpu.with_memory_space_constraint(a, pltpu.HBM)
        for a in (gate_saved, up_saved, out_grad, w_gate, w_up, w_down)
    ]
    tp = lax.axis_size("tp")
    tokens = out_grad.shape[0]
    block = w_gate.shape[0]
    place = lax.axis_index("fs").astype(jnp.int32).reshape(1)
    inputs = jnp.broadcast_to(layer_input.T[None], (tp, block // tp, tokens))
    inputs = lax.all_to_all(inputs, "tp", 0, 0, tiled=True).reshape(block, tokens)
    run = LANES // DOWN_ROWS
    swish, slope, *rest = conv_cells(place, gate_saved, up_saved, conv_taps, out_grad, w_down)
    downs, acts = rest[:run], rest[run:]
    acts = [pltpu.with_memory_space_constraint(a, pltpu.VMEM) for a in lax.psum(acts, "fs")]
    inputs, swish, slope, *downs = [
        pltpu.with_memory_space_constraint(a, pltpu.HBM) for a in (inputs, swish, slope, *downs)
    ]
    terms, taps, *grads = grad_cells(
        conv_taps, swish, slope, gate_saved, inputs, w_gate, w_up, acts, downs
    )
    terms = lax.all_to_all(terms.reshape(tp, block // tp, tokens), "tp", 0, 0, tiled=True)
    input_grad = jnp.sum(terms.astype(jnp.float32), axis=0).astype(jnp.bfloat16).T
    *grads, taps = [
        pltpu.with_memory_space_constraint(a, pltpu.VMEM) for a in lax.psum([*grads, taps], "rep")
    ]
    half = block // ROWS
    groups = [grads[:half], grads[half : 2 * half], grads[2 * half :], [taps]]
    gate_grad, up_grad, down_grad, taps_grad = widened(groups)
    return (input_grad, gate_grad, up_grad, down_grad, taps_grad)


def solution(mesh):
    placed = (
        P("rep", ("fs", "tp")),
        P("rep", "tp"),
        P("rep", "tp"),
        P("rep", None),
        P(None, "tp"),
        P("fs", "tp"),
        P("fs", "tp"),
        P("tp", "fs"),
    )
    return jax.shard_map(
        local,
        mesh=mesh,
        in_specs=placed,
        out_specs=(
            P("rep", ("fs", "tp")),
            P("fs", "tp"),
            P("fs", "tp"),
            P("tp", "fs"),
            P(None, "tp"),
        ),
        check_vma=False,
    )
```

time: 257 us -> 154 us (0.60)
  waiting for transfers between devices: 153 us -> 0.01 us
  blocking collectives: 32 us -> 113 us
  matrix products: 19.9 us -> 0 us
  Pallas kernels: 0 us -> 14.9 us
  between operations: 14.1 us -> 0.67 us
  other arithmetic: 8.8 us -> 0.68 us
  local copies, waits for them, and re-layouts: 6.72 us -> 3.01 us
    psum x1 -> x0, waiting for transfers between devices: 104 us -> none  [local(): lax.psum(token_product(input_block, gate_part).astype(jnp.bfloat16), 'rep')]
    psum x1 -> x2, blocking collectives: 32 us -> 113 us  [the longest x1 74.4 us: local(): lax.psum([*grads, taps], 'rep')]
    all_gather x1 -> x0, waiting for transfers between devices: 47.5 us -> none  [local(): lax.all_gather(w_down, 'fs', axis=1, tiled=True)]
    dot_general x6 -> x0, matrix products: 19.9 us -> none  [the longest x3 13.4 us: width_product(): lax.dot_general(left, right, (((1,), (1,)), ((), ())), preferred_element_...]
    pallas_call x0 -> x3, Pallas kernels: none -> 14.9 us  [the longest x1 7.43 us: grad_cells(): pl.pallas_call(lambda *refs: grad_kernel(counts, *refs), out_shape=out, g...]
    convert_element_type x5 -> x0, other arithmetic: 8.11 us -> none  [the longest x1 2.58 us: swish_cells(): gate_float = gate_cols.astype(jnp.float32)]
    unnamed x24 -> x6, local copies, waits for them, and re-layouts: 4.32 us -> 1.43 us
  transfers between devices with their start and end apart: 4 -> 2, of which waited for: 2 -> 0; matrix products, arithmetic and copies ran while one was open for 9% -> 0% of each run, Pallas kernels for 0% -> 5%
where the time goes in v1:
time: 154 us; the launch traced here: 153 us
  blocking collectives  113 us (73%)
  starting transfers between devices  21.3 us (14%)
  Pallas kernels  14.9 us (10%)
  local copies, waits for them, and re-layouts  3.01 us (2%)
    psum x1, blocking collectives, local(): lax.psum([*grads, taps], 'rep')  74.4 us
    psum x1, blocking collectives, local(): lax.psum(acts, 'fs')  38.3 us
    all_to_all x1, starting transfers between devices, local(): lax.all_to_all(inputs, 'tp', 0, 0, tiled=True).reshape(block, tokens)  16.5 us
    pallas_call x1, Pallas kernels, grad_cells(): pl.pallas_call(lambda *refs: grad_kernel(counts, *refs), out_shape=out, g...  7.43 us
    pallas_call x1, Pallas kernels, conv_cells(): pl.pallas_call(conv_kernel, out_shape=[cells, cells] + [down] * run + act...  5.99 us
    all_to_all x1, starting transfers between devices, local(): lax.all_to_all(terms.reshape(tp, block // tp, tokens), 'tp', 0, 0, tiled=...  4.8 us
  transfers between devices with their start and end apart: 2, of which 0 were waited for; matrix products, arithmetic and copies ran while one was open for 0% of the time, Pallas kernels for 5%

profile of v1, /device:TPU:6, one launch (start us, length us, event | category | flops | bytes accessed | tf_op | source)
XLA Modules:
  0.0 153.3 jit_solution(10465217299768831615)
XLA Ops:
  0.6 1.6 %broadcast_in_dim.2 = bf16[8,32,768]{2,1,0:T(8,128)(2,1)} broadcast(bf16[32,768]{1,0:T(8,128)(2,1)} %bitcast.7), dimensions={1,2} | broadcast | bytes 442368 | tf_op jit(solution)/shard_map/broadcast_in_dim | solution.py:203
  2.2 16.5 %all-to-all-start = ((bf16[8,32,768]{2,1,0:T(8,128)(2,1)}), bf16[8,32,768]{2,1,0:T(8,128)(2,1)S(1)}, u32[]{:S(2)}, u32[]{:S(2)}) async-start(bf16[8,32,768]{2,1,0:T(8,128)(2,1)} %broadcast_in_dim.2), calls=%async_computation | async-start | bytes 786432 | tf_op jit(solution)/shard_map/all_to_all | solution.py:204
  18.7 0.0 copy-start
  18.7 0.7 copy-done
  19.4 0.0 copy-start.1
  19.4 6.0 %conv_cells.1 = (bf16[768,640]{1,0:T(8,128)(2,1)}, bf16[768,640]{1,0:T(8,128)(2,1)}, bf16[160,256]{1,0:T(8,128)(2,1)}, bf16[160,256]{1,0:T(8,128)(2,1)}, bf16[16...) custom-call(s32[1]{0:T(128)} %bitcast.place, ...), custom_call_target="tpu_custom_call" | custom-call | tf_op jit(solution)/shard_map/conv_cells/pallas_call | solution.py:72
  25.4 38.3 %all-reduce.4 = (bf16[8,640]{1,0:T(8,128)(2,1)S(1)}, bf16[8,640]{1,0:T(8,128)(2,1)S(1)}, bf16[8,640]{1,0:T(8,128)(2,1)S(1)}, bf16[8,640]{1,0:T(8,128)(2,1)S(1)},...) all-reduce(bf16[8,640]{1,0:T(8,128)(2,1)S(1)} %get-tuple-element.19, ...), channel_id=1, replica_groups=mesh['rep'=16,'fs'=8,'tp'=8] {'fs'}, use_global_device_ids=true, to_apply=%region_0.0 | all-reduce | flops 491520 | bytes 1966080 | tf_op jit(solution)/shard_map/psum | solution.py:208
  63.7 0.0 all-to-all-done
  63.7 0.0 copy-start.2
  63.8 0.7 copy-done.2
  64.5 0.0 copy-done.1
  64.5 7.4 %grad_cells.1 = (bf16[256,768]{1,0:T(8,128)(2,1)}, bf16[3,640]{1,0:T(4,128)(2,1)S(1)}, bf16[8,640]{1,0:T(8,128)(2,1)S(1)}, bf16[8,640]{1,0:T(8,128)(2,1)S(1)}, b...) custom-call(bf16[3,640]{1,0:T(4,128)(2,1)S(1)} %copy-done.1, ...), custom_call_target="tpu_custom_call" | custom-call | tf_op jit(solution)/shard_map/grad_cells/pallas_call | solution.py:157
  71.9 4.8 %all-to-all-start.1 = ((bf16[8,32,768]{2,1,0:T(8,128)(2,1)}), bf16[8,32,768]{2,1,0:T(8,128)(2,1)S(1)}, u32[]{:S(2)}, u32[]{:S(2)}) async-start(bf16[8,32,768]{2,1,0:T(8,128)(2,1)} %bitcast.6), calls=%async_computation.1 | async-start | bytes 786432 | tf_op jit(solution)/shard_map/all_to_all | solution.py:215
  76.7 74.4 %all-reduce.5 = (bf16[8,640]{1,0:T(8,128)(2,1)S(1)}, bf16[8,640]{1,0:T(8,128)(2,1)S(1)}, bf16[8,640]{1,0:T(8,128)(2,1)S(1)}, bf16[8,640]{1,0:T(8,128)(2,1)S(1)},...) all-reduce(bf16[8,640]{1,0:T(8,128)(2,1)S(1)} %get-tuple-element.30, ...), channel_id=1, replica_groups=mesh['rep'=16,'fs'=8,'tp'=8] {'rep'}, use_global_device_ids=true, to_apply=%region_97.0 | all-reduce | flops 493440 | bytes 1973760 | tf_op jit(solution)/shard_map/psum | solution.py:218
  151.1 1.5 widened.1
  152.6 0.0 all-to-all-done.1
  152.6 0.7 reduce_sum.12
Async XLA Ops:
  2.2 61.5 %all-to-all-start = ((bf16[8,32,768]{2,1,0:T(8,128)(2,1)}), bf16[8,32,768]{2,1,0:T(8,128)(2,1)S(1)}, u32[]{:S(2)}, u32[]{:S(2)}) async-start(bf16[8,32,768]{2,1,0:T(8,128)(2,1)} %broadcast_in_dim.2), calls=%async_computation | async-start | bytes 786432 | tf_op jit(solution)/shard_map/all_to_all | solution.py:204
  18.7 0.7 copy-start
  19.4 45.1 %copy-start.1 = (bf16[3,640]{1,0:T(4,128)(2,1)S(1)}, bf16[3,640]{1,0:T(4,128)(2,1)}, u32[]{:S(2)}) copy-start(bf16[3,640]{1,0:T(4,128)(2,1)} %refs_0_.1) | copy-start | bytes 11524
  63.7 0.7 copy-start.2
  71.9 80.7 %all-to-all-start.1 = ((bf16[8,32,768]{2,1,0:T(8,128)(2,1)}), bf16[8,32,768]{2,1,0:T(8,128)(2,1)S(1)}, u32[]{:S(2)}, u32[]{:S(2)}) async-start(bf16[8,32,768]{2,1,0:T(8,128)(2,1)} %bitcast.6), calls=%async_computation.1 | async-start | bytes 786432 | tf_op jit(solution)/shard_map/all_to_all | solution.py:215

commit v2 on v1

--- a/solution.py
+++ b/solution.py
@@ -6,8 +6,8 @@
 from jax.sharding import PartitionSpec as P
 
 LANES = 128
-ROWS = 8
-DOWN_ROWS = 32
+ROWS = 48
+DOWN_ROWS = 64
 TAPS = 3
 
 
@@ -26,14 +26,17 @@
     return pl.ds(pl.multiple_of(c * LANES, LANES), LANES)
 
 
-def split_rows(out, values):
-    rows = out[0].shape[0]
-    for i, ref in enumerate(out):
-        ref[...] = values[i * rows : (i + 1) * rows]
+def split_rows(out, values, lanes=slice(None)):
+    start = 0
+    for ref in out:
+        rows = ref.shape[0]
+        ref[:, lanes] = values[start : start + rows]
+        start += rows
 
 
 def slabs(length, rows, width):
-    return [pltpu.VMEM((rows, width), jnp.bfloat16)] * (length // rows)
+    starts = range(0, length, rows)
+    return [pltpu.VMEM((min(rows, length - s), width), jnp.bfloat16) for s in starts]
 
 
 def whole(array):
@@ -43,8 +46,7 @@
 def conv_kernel(place, gate, up, taps, grad, down, swish_out, slope_out, *refs):
     down_out, act_out = refs[: LANES // DOWN_ROWS], refs[LANES // DOWN_ROWS :]
     share = product(grad[...], down[...], ((1,), (1,))).astype(jnp.bfloat16)
-    for i, ref in enumerate(act_out):
-        ref[:, lanes_of(pl.program_id(0))] = share[i * ROWS : (i + 1) * ROWS]
+    split_rows(act_out, share, lanes_of(pl.program_id(0)))
     gate_float = gate[...].astype(jnp.float32)
     up_float = up[...].astype(jnp.float32)
     taps_float = taps[...].astype(jnp.float32)
@@ -100,7 +102,7 @@
 
 
 def grad_kernel(counts, taps, swish, slope, gate, inputs, w_gate, w_up, *refs):
-    acts, downs, (terms_out, taps_out), gate_out, up_out, down_out, (terms,) = taken(refs, counts)
+    acts, downs, _, (terms_out, taps_out), grads_out, down_out, (terms,) = taken(refs, counts)
     c = pl.program_id(0)
     for i, down in enumerate(downs):
         for j in range(len(down_out) // len(downs)):
@@ -123,11 +125,11 @@
         for ahead in (ahead_two, ahead_one, conv_grad)
     ]
     taps_out[:, lanes_of(c)] = jnp.concatenate(sums, 0).astype(jnp.bfloat16)
-    for out, part in ((gate_out, gate_part), (up_out, up_part)):
-        grads = product(inputs[...], part, ((1,), (0,))).astype(jnp.bfloat16)
-        for i, ref in enumerate(out):
-            ref[:, lanes_of(c)] = grads[i * ROWS : (i + 1) * ROWS]
-    term = product(w_gate[...], gate_part, ((1,), (1,))) + product(w_up[...], up_part, ((1,), (1,)))
+    parts = jnp.concatenate([gate_part, up_part], 1)
+    grads = product(inputs[...], parts, ((1,), (0,))).astype(jnp.bfloat16)
+    split_rows(grads_out, jnp.concatenate([grads[:, :LANES], grads[:, LANES:]], 0), lanes_of(c))
+    weights = jnp.concatenate([w_gate[...], w_up[...]], 1)
+    term = product(weights, parts, ((1,), (1,)))
 
     @pl.when(c == 0)
     def first():
@@ -142,18 +144,18 @@
         terms_out[...] = terms[...].astype(jnp.bfloat16)
 
 
-def grad_cells(conv_taps, swish, slope, gate_saved, inputs, w_gate, w_up, acts, downs):
+def grad_cells(conv_taps, swish, slope, gate_saved, inputs, w_gate, w_up, acts, downs, extra):
     tokens, hidden = swish.shape
     block = inputs.shape[0]
     columns = pl.BlockSpec((tokens, LANES), lambda c: (0, c))
     weights = pl.BlockSpec((block, LANES), lambda c: (0, c))
-    grads = slabs(block, ROWS, hidden)
+    grads = slabs(2 * block, ROWS, hidden)
     kept = slabs(hidden, DOWN_ROWS, block)
     out = [
         pltpu.HBM((block, tokens), jnp.bfloat16),
         pltpu.VMEM((TAPS, hidden), jnp.bfloat16),
-    ] + grads * 2 + kept
-    counts = [len(acts), len(downs), 2, len(grads), len(grads), len(kept)]
+    ] + grads + kept
+    counts = [len(acts), len(downs), 1, 2, len(grads), len(kept)]
     return pl.pallas_call(
         lambda *refs: grad_kernel(counts, *refs),
         out_shape=out,
@@ -161,34 +163,51 @@
         in_specs=[pl.BlockSpec((TAPS, LANES), lambda c: (0, c)), columns, columns, columns]
         + [whole(inputs), weights, weights]
         + [whole(a) for a in acts]
-        + [pl.BlockSpec((DOWN_ROWS, block), lambda c: (c, 0))] * len(downs),
+        + [pl.BlockSpec((DOWN_ROWS, block), lambda c: (c, 0))] * len(downs)
+        + [pl.BlockSpec(memory_space=pl.ANY)],
         out_specs=[whole(o) for o in out],
         scratch_shapes=[pltpu.VMEM((block, tokens), jnp.float32)],
         compiler_params=pltpu.CompilerParams(vmem_limit_bytes=24 << 20),
         name="grad_cells",
-    )(conv_taps, swish, slope, gate_saved, inputs, w_gate, w_up, *acts, *downs)
+    )(conv_taps, swish, slope, gate_saved, inputs, w_gate, w_up, *acts, *downs, extra)
 
 
 def widen_kernel(counts, *refs):
-    ins, outs = refs[: sum(counts)], refs[sum(counts) :]
-    for out, count in zip(outs, counts):
-        rows = out.shape[0] // count
-        for i, ref in enumerate(ins[:count]):
-            out[i * rows : (i + 1) * rows, :] = ref[...].astype(jnp.float32)
-        ins = ins[count:]
-
-
-def widened(groups):
-    out = [
-        jax.ShapeDtypeStruct((sum(a.shape[0] for a in g), g[0].shape[1]), jnp.float32)
-        for g in groups
-    ]
+    pairs, downs, (taps, _), (gate_out, up_out, down_out, taps_out) = taken(refs, counts)
+    block = gate_out.shape[0]
+    start = 0
+    for ref in pairs:
+        rows = ref.shape[0]
+        values = ref[...].astype(jnp.float32)
+        cut = min(max(block - start, 0), rows)
+        if cut > 0:
+            gate_out[start : start + cut, :] = values[:cut]
+        if cut < rows:
+            up_out[start + cut - block : start + rows - block, :] = values[cut:]
+        start += rows
+    for i, ref in enumerate(downs):
+        down_out[i * DOWN_ROWS : (i + 1) * DOWN_ROWS, :] = ref[...].astype(jnp.float32)
+    taps_out[...] = taps[...].astype(jnp.float32)
+
+
+def widened(pairs, downs, taps, extra):
+    hidden = taps.shape[1]
+    block = downs[0].shape[1]
+    grads = jax.ShapeDtypeStruct((block, hidden), jnp.float32)
+    counts = [len(pairs), len(downs), 2]
     return pl.pallas_call(
-        lambda *refs: widen_kernel([len(g) for g in groups], *refs),
-        out_shape=out,
+        lambda *refs: widen_kernel(counts, *refs),
+        out_shape=[
+            grads,
+            grads,
+            jax.ShapeDtypeStruct((hidden, block), jnp.float32),
+            jax.ShapeDtypeStruct((TAPS, hidden), jnp.float32),
+        ],
+        in_specs=[pl.BlockSpec(memory_space=pltpu.VMEM)] * (sum(counts) - 1)
+        + [pl.BlockSpec(memory_space=pl.ANY)],
         compiler_params=pltpu.CompilerParams(vmem_limit_bytes=16 << 20),
         name="widened",
-    )(*[a for g in groups for a in g])
+    )(*pairs, *downs, taps, extra)
 
 
 def local(layer_input, gate_saved, up_saved, out_grad, conv_taps, w_gate, w_up, w_down):
@@ -205,21 +224,23 @@
     run = LANES // DOWN_ROWS
     swish, slope, *rest = conv_cells(place, gate_saved, up_saved, conv_taps, out_grad, w_down)
     downs, acts = rest[:run], rest[run:]
-    acts = [pltpu.with_memory_space_constraint(a, pltpu.VMEM) for a in lax.psum(acts, "fs")]
+    scalar = conv_taps[0, 0]
+    *acts, extra = lax.psum([*acts, scalar], "fs")
+    acts = [pltpu.with_memory_space_constraint(a, pltpu.VMEM) for a in acts]
     inputs, swish, slope, *downs = [
         pltpu.with_memory_space_constraint(a, pltpu.HBM) for a in (inputs, swish, slope, *downs)
     ]
     terms, taps, *grads = grad_cells(
-        conv_taps, swish, slope, gate_saved, inputs, w_gate, w_up, acts, downs
+        conv_taps, swish, slope, gate_saved, inputs, w_gate, w_up, acts, downs, extra.reshape(1, 1)
     )
     terms = lax.all_to_all(terms.reshape(tp, block // tp, tokens), "tp", 0, 0, tiled=True)
     input_grad = jnp.sum(terms.astype(jnp.float32), axis=0).astype(jnp.bfloat16).T
-    *grads, taps = [
-        pltpu.with_memory_space_constraint(a, pltpu.VMEM) for a in lax.psum([*grads, taps], "rep")
-    ]
-    half = block // ROWS
-    groups = [grads[:half], grads[half : 2 * half], grads[2 * half :], [taps]]
-    gate_grad, up_grad, down_grad, taps_grad = widened(groups)
+    *grads, taps, extra = lax.psum([*grads, taps, scalar], "rep")
+    *grads, taps = [pltpu.with_memory_space_constraint(a, pltpu.VMEM) for a in (*grads, taps)]
+    count = -(-2 * block // ROWS)
+    gate_grad, up_grad, down_grad, taps_grad = widened(
+        grads[:count], grads[count:], taps, extra.reshape(1, 1)
+    )
     return (input_grad, gate_grad, up_grad, down_grad, taps_grad)
 
 

time: 154 us -> 154 us (level)
  blocking collectives: 113 us -> 111 us
    psum x2, blocking collectives: 113 us -> 111 us  [the longest x1 74.1 us: local(): *grads, taps, extra = lax.psum([*grads, taps, scalar], 'rep')]
  transfers between devices with their start and end apart: 2 -> 2, of which waited for: 0 -> 0; matrix products, arithmetic and copies ran while one was open for 0% -> 1% of each run, Pallas kernels for 5% -> 5%
where the time goes in v2:
time: 154 us; the launch traced here: 153 us
  blocking collectives  111 us (72%)
  starting transfers between devices  21.3 us (14%)
  Pallas kernels  15.2 us (10%)
  local copies, waits for them, and re-layouts  4.2 us (3%)
    psum x1, blocking collectives, local(): *grads, taps, extra = lax.psum([*grads, taps, scalar], 'rep')  74.1 us
    psum x1, blocking collectives, local(): *acts, extra = lax.psum([*acts, scalar], 'fs')  37 us
    all_to_all x1, starting transfers between devices, local(): lax.all_to_all(inputs, 'tp', 0, 0, tiled=True).reshape(block, tokens)  16.5 us
    pallas_call x1, Pallas kernels, grad_cells(): pl.pallas_call(lambda *refs: grad_kernel(counts, *refs), out_shape=out, g...  7.31 us
    pallas_call x1, Pallas kernels, conv_cells(): pl.pallas_call(conv_kernel, out_shape=[cells, cells] + [down] * run + act...  5.86 us
    all_to_all x1, starting transfers between devices, local(): lax.all_to_all(terms.reshape(tp, block // tp, tokens), 'tp', 0, 0, tiled=...  4.79 us
  transfers between devices with their start and end apart: 2, of which 0 were waited for; matrix products, arithmetic and copies ran while one was open for 1% of the time, Pallas kernels for 5%

profile of v2, /device:TPU:6, one launch (start us, length us, event | category | flops | bytes accessed | tf_op | source)
XLA Modules:
  0.0 153.2 jit_solution(15903709698203649686)
XLA Ops:
  0.6 1.6 %broadcast_in_dim.2 = bf16[8,32,768]{2,1,0:T(8,128)(2,1)} broadcast(bf16[32,768]{1,0:T(8,128)(2,1)} %bitcast.7), dimensions={1,2} | broadcast | bytes 442368 | tf_op jit(solution)/shard_map/broadcast_in_dim | solution.py:222
  2.2 16.5 %all-to-all-start = ((bf16[8,32,768]{2,1,0:T(8,128)(2,1)}), bf16[8,32,768]{2,1,0:T(8,128)(2,1)S(1)}, u32[]{:S(2)}, u32[]{:S(2)}) async-start(bf16[8,32,768]{2,1,0:T(8,128)(2,1)} %broadcast_in_dim.2), calls=%async_computation | async-start | bytes 786432 | tf_op jit(solution)/shard_map/all_to_all | solution.py:223
  18.7 1.2 slice.3
  19.9 0.0 copy-start
  19.9 0.7 copy-done
  20.6 0.0 copy-start.1
  20.6 5.9 %conv_cells.1 = (bf16[768,640]{1,0:T(8,128)(2,1)}, bf16[768,640]{1,0:T(8,128)(2,1)}, bf16[320,256]{1,0:T(8,128)(2,1)}, bf16[320,256]{1,0:T(8,128)(2,1)}, bf16[48...) custom-call(s32[1]{0:T(128)} %bitcast.place, ...), custom_call_target="tpu_custom_call" | custom-call | tf_op jit(solution)/shard_map/conv_cells/pallas_call | solution.py:74
  26.4 37.0 %all-reduce.4 = (bf16[48,640]{1,0:T(8,128)(2,1)S(1)}, bf16[48,640]{1,0:T(8,128)(2,1)S(1)}, bf16[48,640]{1,0:T(8,128)(2,1)S(1)}, bf16[48,640]{1,0:T(8,128)(2,1)S(...) all-reduce(bf16[48,640]{1,0:T(8,128)(2,1)S(1)} %get-tuple-element.5, ...), channel_id=1, replica_groups=mesh['rep'=16,'fs'=8,'tp'=8] {'fs'}, use_global_device_ids=true, to_apply=%region_0.0 | all-reduce | flops 491521 | bytes 1966084 | tf_op jit(solution)/shard_map/psum | solution.py:228
  63.5 0.0 all-to-all-done
  63.5 0.0 copy-start.2
  63.5 0.7 copy-done.2
  64.2 0.0 copy-done.1
  64.2 7.3 %grad_cells.1 = (bf16[256,768]{1,0:T(8,128)(2,1)}, bf16[3,640]{1,0:T(4,128)(2,1)S(1)}, bf16[48,640]{1,0:T(8,128)(2,1)S(1)}, bf16[48,640]{1,0:T(8,128)(2,1)S(1)},...) custom-call(bf16[3,640]{1,0:T(4,128)(2,1)S(1)} %copy-done.1, ...), custom_call_target="tpu_custom_call" | custom-call | tf_op jit(solution)/shard_map/grad_cells/pallas_call | solution.py:159
  71.5 4.8 %all-to-all-start.1 = ((bf16[8,32,768]{2,1,0:T(8,128)(2,1)}), bf16[8,32,768]{2,1,0:T(8,128)(2,1)S(1)}, u32[]{:S(2)}, u32[]{:S(2)}) async-start(bf16[8,32,768]{2,1,0:T(8,128)(2,1)} %bitcast.6), calls=%async_computation.1 | async-start | bytes 786432 | tf_op jit(solution)/shard_map/all_to_all | solution.py:236
  76.3 74.1 %all-reduce.5 = (bf16[48,640]{1,0:T(8,128)(2,1)S(1)}, bf16[48,640]{1,0:T(8,128)(2,1)S(1)}, bf16[48,640]{1,0:T(8,128)(2,1)S(1)}, bf16[48,640]{1,0:T(8,128)(2,1)S(...) all-reduce(bf16[48,640]{1,0:T(8,128)(2,1)S(1)} %get-tuple-element.7, ...), channel_id=1, replica_groups=mesh['rep'=16,'fs'=8,'tp'=8] {'rep'}, use_global_device_ids=true, to_apply=%region_18.0 | all-reduce | flops 493441 | bytes 1973764 | tf_op jit(solution)/shard_map/psum | solution.py:238
  150.5 2.0 %widened.1 = (f32[256,640]{1,0:T(8,128)}, f32[256,640]{1,0:T(8,128)}, f32[640,256]{1,0:T(8,128)}, f32[3,640]{1,0:T(4,128)}) custom-call(bf16[48,640]{1,0:T(8,128)(2,1)S(1)} %get-tuple-element.99.refs_0_, bf16[48,640]{1,0:T(8,128)(2,1)S(1)} %get-tuple-element.100.refs_1_, bf16[48,640]{1,0:T(8,128)(2,1)S(1)} %get-tuple-element.101.refs_2_, ...), custom_call_target="tpu_custom_call" | custom-call | tf_op jit(solution)/shard_map/widened/pallas_call | solution.py:198
  152.5 0.0 all-to-all-done.1
  152.5 0.7 reduce_sum.12
Async XLA Ops:
  2.2 61.3 %all-to-all-start = ((bf16[8,32,768]{2,1,0:T(8,128)(2,1)}), bf16[8,32,768]{2,1,0:T(8,128)(2,1)S(1)}, u32[]{:S(2)}, u32[]{:S(2)}) async-start(bf16[8,32,768]{2,1,0:T(8,128)(2,1)} %broadcast_in_dim.2), calls=%async_computation | async-start | bytes 786432 | tf_op jit(solution)/shard_map/all_to_all | solution.py:223
  19.9 0.7 copy-start
  20.6 43.7 %copy-start.1 = (bf16[3,640]{1,0:T(4,128)(2,1)S(1)}, bf16[3,640]{1,0:T(4,128)(2,1)}, u32[]{:S(2)}) copy-start(bf16[3,640]{1,0:T(4,128)(2,1)} %refs_0_.1) | copy-start | bytes 11524
  63.5 0.7 copy-start.2
  71.5 80.9 %all-to-all-start.1 = ((bf16[8,32,768]{2,1,0:T(8,128)(2,1)}), bf16[8,32,768]{2,1,0:T(8,128)(2,1)S(1)}, u32[]{:S(2)}, u32[]{:S(2)}) async-start(bf16[8,32,768]{2,1,0:T(8,128)(2,1)} %bitcast.6), calls=%async_computation.1 | async-start | bytes 786432 | tf_op jit(solution)/shard_map/all_to_all | solution.py:236

commit v3 on v2

--- a/solution.py
+++ b/solution.py
@@ -17,9 +17,11 @@
 
 def moved(values, count):
     tokens = values.shape[0]
-    row = lax.broadcasted_iota(jnp.int32, values.shape, 0)
-    inside = (row >= count) if count > 0 else (row < tokens + count)
-    return jnp.where(inside, pltpu.roll(values, count % tokens, 0), 0.0)
+    turned = pltpu.roll(values, count % tokens, 0)
+    row = lax.broadcasted_iota(jnp.int32, (8, values.shape[1]), 0)
+    if count > 0:
+        return jnp.concatenate([jnp.where(row >= count, turned[:8], 0.0), turned[8:]], 0)
+    return jnp.concatenate([turned[:-8], jnp.where(row < 8 + count, turned[-8:], 0.0)], 0)
 
 
 def lanes_of(c):
@@ -43,8 +45,16 @@
     return pl.BlockSpec(array.shape, lambda c, *_: (0,) * len(array.shape))
 
 
-def conv_kernel(place, gate, up, taps, grad, down, swish_out, slope_out, *refs):
-    down_out, act_out = refs[: LANES // DOWN_ROWS], refs[LANES // DOWN_ROWS :]
+def conv_kernel(place, gate, up, taps, grad, down, inputs, *refs):
+    swish_out, slope_out, copies_out, one_out = refs[:4]
+    down_out, act_out = refs[4 : 4 + LANES // DOWN_ROWS], refs[4 + LANES // DOWN_ROWS :]
+
+    @pl.when(pl.program_id(0) == 0)
+    def first():
+        one_out[...] = taps[0:1, 0:1]
+        for i in range(copies_out.shape[0]):
+            copies_out[i] = inputs[...]
+
     share = product(grad[...], down[...], ((1,), (1,))).astype(jnp.bfloat16)
     split_rows(act_out, share, lanes_of(pl.program_id(0)))
     gate_float = gate[...].astype(jnp.float32)
@@ -55,25 +65,27 @@
         + taps_float[1:2] * moved(gate_float, 1)
         + taps_float[2:3] * gate_float
     )
-    sig = jax.nn.sigmoid(conv_out)
+    sig = 0.5 * jnp.tanh(0.5 * conv_out) + 0.5
     swish = conv_out * sig
     swish_out[...] = swish.astype(jnp.bfloat16)
-    slope_out[...] = (up_float * sig * (1.0 + conv_out * (1.0 - sig))).astype(jnp.bfloat16)
+    slope_out[...] = (up_float * (sig + swish * (1.0 - sig))).astype(jnp.bfloat16)
     activation = (swish * up_float).astype(jnp.bfloat16)
     split_rows(down_out, product(activation, grad[...], ((0,), (0,))).astype(jnp.bfloat16))
 
 
-def conv_cells(place, gate_saved, up_saved, conv_taps, out_grad, w_down):
+def conv_cells(place, gate_saved, up_saved, conv_taps, out_grad, w_down, inputs, copies):
     tokens, hidden = gate_saved.shape
     block = w_down.shape[1]
     acts = slabs(tokens, ROWS, hidden)
     columns = pl.BlockSpec((tokens, LANES), lambda c, s: (0, c))
     cells = pltpu.HBM((tokens, hidden), jnp.bfloat16)
+    copies = pltpu.HBM((copies, *inputs.shape), inputs.dtype)
+    one = jax.ShapeDtypeStruct((1, 1), jnp.bfloat16)
     run = LANES // DOWN_ROWS
     down = pltpu.HBM((hidden // run, block), jnp.bfloat16)
     return pl.pallas_call(
         conv_kernel,
-        out_shape=[cells, cells] + [down] * run + acts,
+        out_shape=[cells, cells, copies, one] + [down] * run + acts,
         grid_spec=pltpu.PrefetchScalarGridSpec(
             num_scalar_prefetch=1,
             grid=(hidden // LANES,),
@@ -83,14 +95,15 @@
                 pl.BlockSpec((TAPS, LANES), lambda c, s: (0, c)),
                 pl.BlockSpec((tokens, block), lambda c, s: (0, s[0])),
                 pl.BlockSpec((LANES, block), lambda c, s: (c, 0)),
+                whole(inputs),
             ],
-            out_specs=[columns, columns]
+            out_specs=[columns, columns, whole(copies), whole(one)]
             + [pl.BlockSpec((DOWN_ROWS, block), lambda c, s: (c, 0))] * run
             + [whole(a) for a in acts],
         ),
         compiler_params=pltpu.CompilerParams(vmem_limit_bytes=16 << 20),
         name="conv_cells",
-    )(place, gate_saved, up_saved, conv_taps, out_grad, w_down)
+    )(place, gate_saved, up_saved, conv_taps, out_grad, w_down, inputs)
 
 
 def taken(refs, counts):
@@ -211,35 +224,36 @@
 
 
 def local(layer_input, gate_saved, up_saved, out_grad, conv_taps, w_gate, w_up, w_down):
-    gate_saved, up_saved, out_grad, w_gate, w_up, w_down = [
+    layer_input, gate_saved, up_saved, out_grad, conv_taps, w_gate, w_up, w_down = [
         pltpu.with_memory_space_constraint(a, pltpu.HBM)
-        for a in (gate_saved, up_saved, out_grad, w_gate, w_up, w_down)
+        for a in (layer_input.T, gate_saved, up_saved, out_grad, conv_taps, w_gate, w_up, w_down)
     ]
     tp = lax.axis_size("tp")
     tokens = out_grad.shape[0]
     block = w_gate.shape[0]
     place = lax.axis_index("fs").astype(jnp.int32).reshape(1)
-    inputs = jnp.broadcast_to(layer_input.T[None], (tp, block // tp, tokens))
-    inputs = lax.all_to_all(inputs, "tp", 0, 0, tiled=True).reshape(block, tokens)
     run = LANES // DOWN_ROWS
-    swish, slope, *rest = conv_cells(place, gate_saved, up_saved, conv_taps, out_grad, w_down)
+    swish, slope, copies, one, *rest = conv_cells(
+        place, gate_saved, up_saved, conv_taps, out_grad, w_down, layer_input, tp
+    )
     downs, acts = rest[:run], rest[run:]
-    scalar = conv_taps[0, 0]
-    *acts, extra = lax.psum([*acts, scalar], "fs")
+    inputs = lax.all_to_all(copies, "tp", 0, 0, tiled=True).reshape(block, tokens)
+    *acts, extra = lax.psum([*acts, one], "fs")
     acts = [pltpu.with_memory_space_constraint(a, pltpu.VMEM) for a in acts]
-    inputs, swish, slope, *downs = [
-        pltpu.with_memory_space_constraint(a, pltpu.HBM) for a in (inputs, swish, slope, *downs)
+    inputs = pltpu.with_memory_space_constraint(inputs, pltpu.VMEM)
+    swish, slope, *downs = [
+        pltpu.with_memory_space_constraint(a, pltpu.HBM) for a in (swish, slope, *downs)
     ]
     terms, taps, *grads = grad_cells(
-        conv_taps, swish, slope, gate_saved, inputs, w_gate, w_up, acts, downs, extra.reshape(1, 1)
+        conv_taps, swish, slope, gate_saved, inputs, w_gate, w_up, acts, downs, extra
     )
     terms = lax.all_to_all(terms.reshape(tp, block // tp, tokens), "tp", 0, 0, tiled=True)
     input_grad = jnp.sum(terms.astype(jnp.float32), axis=0).astype(jnp.bfloat16).T
-    *grads, taps, extra = lax.psum([*grads, taps, scalar], "rep")
+    *grads, taps, extra = lax.psum([*grads, taps, one], "rep")
     *grads, taps = [pltpu.with_memory_space_constraint(a, pltpu.VMEM) for a in (*grads, taps)]
     count = -(-2 * block // ROWS)
     gate_grad, up_grad, down_grad, taps_grad = widened(
-        grads[:count], grads[count:], taps, extra.reshape(1, 1)
+        grads[:count], grads[count:], taps, extra
     )
     return (input_grad, gate_grad, up_grad, down_grad, taps_grad)
 

time: 154 us -> 150 us (0.974)
  local copies, waits for them, and re-layouts: 4.2 us -> 0 us
    broadcast_in_dim x1 -> x0, local copies, waits for them, and re-layouts: 1.57 us -> none  [local(): inputs = jnp.broadcast_to(layer_input.T[None], (tp, block // tp, tokens))]
  transfers between devices with their start and end apart: 2 -> 2, of which waited for: 0 -> 0; matrix products, arithmetic and copies ran while one was open for 1% -> 0% of each run, Pallas kernels for 5% -> 1%
where the time goes in v3:
time: 150 us; the launch traced here: 149 us
  blocking collectives  111 us (74%)
  starting transfers between devices  21.3 us (14%)
  Pallas kernels  15.1 us (10%)
    psum x1, blocking collectives, local(): *grads, taps, extra = lax.psum([*grads, taps, one], 'rep')  74.2 us
    psum x1, blocking collectives, local(): *acts, extra = lax.psum([*acts, one], 'fs')  37 us
    all_to_all x1, starting transfers between devices, local(): lax.all_to_all(copies, 'tp', 0, 0, tiled=True).reshape(block, tokens)  16.5 us
    pallas_call x1, Pallas kernels, grad_cells(): pl.pallas_call(lambda *refs: grad_kernel(counts, *refs), out_shape=out, g...  6.98 us
    pallas_call x1, Pallas kernels, conv_cells(): pl.pallas_call(conv_kernel, out_shape=[cells, cells, copies, one] + [down...  6.07 us
    all_to_all x1, starting transfers between devices, local(): lax.all_to_all(terms.reshape(tp, block // tp, tokens), 'tp', 0, 0, tiled=...  4.79 us
  transfers between devices with their start and end apart: 2, of which 0 were waited for; matrix products, arithmetic and copies ran while one was open for 0% of the time, Pallas kernels for 1%

profile of v3, /device:TPU:6, one launch (start us, length us, event | category | flops | bytes accessed | tf_op | source)
XLA Modules:
  0.0 148.8 jit_solution(15002352801486074949)
XLA Ops:
  0.6 6.1 %conv_cells.1 = (bf16[768,640]{1,0:T(8,128)(2,1)}, bf16[768,640]{1,0:T(8,128)(2,1)}, bf16[8,32,768]{2,1,0:T(8,128)(2,1)}, bf16[1,1]{1,0:T(2,128)(2,1)}, bf16[320...) custom-call(s32[1]{0:T(128)} %bitcast.place, ...), custom_call_target="tpu_custom_call" | custom-call | tf_op jit(solution)/shard_map/conv_cells/pallas_call | solution.py:86
  6.7 16.5 %all-to-all-start = ((bf16[8,32,768]{2,1,0:T(8,128)(2,1)}), bf16[8,32,768]{2,1,0:T(8,128)(2,1)S(1)}, u32[]{:S(2)}, u32[]{:S(2)}) async-start(bf16[8,32,768]{2,1,0:T(8,128)(2,1)} %get-tuple-element.56), calls=%async_computation | async-start | bytes 786432 | tf_op jit(solution)/shard_map/all_to_all | solution.py:240
  23.2 37.0 %all-reduce.4 = (bf16[48,640]{1,0:T(8,128)(2,1)S(1)}, bf16[48,640]{1,0:T(8,128)(2,1)S(1)}, bf16[48,640]{1,0:T(8,128)(2,1)S(1)}, bf16[48,640]{1,0:T(8,128)(2,1)S(...) all-reduce(bf16[48,640]{1,0:T(8,128)(2,1)S(1)} %get-tuple-element.5, ...), channel_id=1, replica_groups=mesh['rep'=16,'fs'=8,'tp'=8] {'fs'}, use_global_device_ids=true, to_apply=%region_0.0 | all-reduce | flops 491521 | bytes 1966084 | tf_op jit(solution)/shard_map/psum | solution.py:241
  60.2 0.0 all-to-all-done
  60.2 7.0 %grad_cells.1 = (bf16[256,768]{1,0:T(8,128)(2,1)}, bf16[3,640]{1,0:T(4,128)(2,1)S(1)}, bf16[48,640]{1,0:T(8,128)(2,1)S(1)}, bf16[48,640]{1,0:T(8,128)(2,1)S(1)},...) custom-call(bf16[3,640]{1,0:T(4,128)(2,1)} %refs_0_.1, ...), custom_call_target="tpu_custom_call" | custom-call | tf_op jit(solution)/shard_map/grad_cells/pallas_call | solution.py:172
  67.2 4.8 %all-to-all-start.1 = ((bf16[8,32,768]{2,1,0:T(8,128)(2,1)}), bf16[8,32,768]{2,1,0:T(8,128)(2,1)S(1)}, u32[]{:S(2)}, u32[]{:S(2)}) async-start(bf16[8,32,768]{2,1,0:T(8,128)(2,1)} %bitcast.6), calls=%async_computation.1 | async-start | bytes 786432 | tf_op jit(solution)/shard_map/all_to_all | solution.py:250
  71.9 74.2 %all-reduce.5 = (bf16[48,640]{1,0:T(8,128)(2,1)S(1)}, bf16[48,640]{1,0:T(8,128)(2,1)S(1)}, bf16[48,640]{1,0:T(8,128)(2,1)S(1)}, bf16[48,640]{1,0:T(8,128)(2,1)S(...) all-reduce(bf16[48,640]{1,0:T(8,128)(2,1)S(1)} %get-tuple-element.7, ...), channel_id=1, replica_groups=mesh['rep'=16,'fs'=8,'tp'=8] {'rep'}, use_global_device_ids=true, to_apply=%region_18.0 | all-reduce | flops 493441 | bytes 1973764 | tf_op jit(solution)/shard_map/psum | solution.py:252
  146.1 2.0 %widened.1 = (f32[256,640]{1,0:T(8,128)}, f32[256,640]{1,0:T(8,128)}, f32[640,256]{1,0:T(8,128)}, f32[3,640]{1,0:T(4,128)}) custom-call(bf16[48,640]{1,0:T(8,128)(2,1)S(1)} %get-tuple-element.103.refs_0_, bf16[48,640]{1,0:T(8,128)(2,1)S(1)} %get-tuple-element.104.refs_1_, bf16[48,640]{1,0:T(8,128)(2,1)S(1)} %get-tuple-element.105.refs_2_, ...), custom_call_target="tpu_custom_call" | custom-call | tf_op jit(solution)/shard_map/widened/pallas_call | solution.py:211
  148.1 0.0 all-to-all-done.1
  148.1 0.7 reduce_sum.12
Async XLA Ops:
  6.7 53.5 %all-to-all-start = ((bf16[8,32,768]{2,1,0:T(8,128)(2,1)}), bf16[8,32,768]{2,1,0:T(8,128)(2,1)S(1)}, u32[]{:S(2)}, u32[]{:S(2)}) async-start(bf16[8,32,768]{2,1,0:T(8,128)(2,1)} %get-tuple-element.56), calls=%async_computation | async-start | bytes 786432 | tf_op jit(solution)/shard_map/all_to_all | solution.py:240
  67.2 81.0 %all-to-all-start.1 = ((bf16[8,32,768]{2,1,0:T(8,128)(2,1)}), bf16[8,32,768]{2,1,0:T(8,128)(2,1)S(1)}, u32[]{:S(2)}, u32[]{:S(2)}) async-start(bf16[8,32,768]{2,1,0:T(8,128)(2,1)} %bitcast.6), calls=%async_computation.1 | async-start | bytes 786432 | tf_op jit(solution)/shard_map/all_to_all | solution.py:250

commit v4 on v3

--- a/solution.py
+++ b/solution.py
@@ -7,7 +7,7 @@
 
 LANES = 128
 ROWS = 48
-DOWN_ROWS = 64
+DOWN_ROWS = 120
 TAPS = 3
 
 
@@ -32,7 +32,7 @@
     start = 0
     for ref in out:
         rows = ref.shape[0]
-        ref[:, lanes] = values[start : start + rows]
+        ref[:, lanes] = values[start : start + rows, :]
         start += rows
 
 
@@ -46,8 +46,7 @@
 
 
 def conv_kernel(place, gate, up, taps, grad, down, inputs, *refs):
-    swish_out, slope_out, copies_out, one_out = refs[:4]
-    down_out, act_out = refs[4 : 4 + LANES // DOWN_ROWS], refs[4 + LANES // DOWN_ROWS :]
+    swish_out, slope_out, copies_out, one_out, down_out, *act_out = refs
 
     @pl.when(pl.program_id(0) == 0)
     def first():
@@ -70,7 +69,7 @@
     swish_out[...] = swish.astype(jnp.bfloat16)
     slope_out[...] = (up_float * (sig + swish * (1.0 - sig))).astype(jnp.bfloat16)
     activation = (swish * up_float).astype(jnp.bfloat16)
-    split_rows(down_out, product(activation, grad[...], ((0,), (0,))).astype(jnp.bfloat16))
+    down_out[...] = product(activation, grad[...], ((0,), (0,))).astype(jnp.bfloat16)
 
 
 def conv_cells(place, gate_saved, up_saved, conv_taps, out_grad, w_down, inputs, copies):
@@ -81,11 +80,10 @@
     cells = pltpu.HBM((tokens, hidden), jnp.bfloat16)
     copies = pltpu.HBM((copies, *inputs.shape), inputs.dtype)
     one = jax.ShapeDtypeStruct((1, 1), jnp.bfloat16)
-    run = LANES // DOWN_ROWS
-    down = pltpu.HBM((hidden // run, block), jnp.bfloat16)
+    down = pltpu.HBM((hidden, block), jnp.bfloat16)
     return pl.pallas_call(
         conv_kernel,
-        out_shape=[cells, cells, copies, one] + [down] * run + acts,
+        out_shape=[cells, cells, copies, one, down] + acts,
         grid_spec=pltpu.PrefetchScalarGridSpec(
             num_scalar_prefetch=1,
             grid=(hidden // LANES,),
@@ -98,7 +96,7 @@
                 whole(inputs),
             ],
             out_specs=[columns, columns, whole(copies), whole(one)]
-            + [pl.BlockSpec((DOWN_ROWS, block), lambda c, s: (c, 0))] * run
+            + [pl.BlockSpec((LANES, block), lambda c, s: (c, 0))]
             + [whole(a) for a in acts],
         ),
         compiler_params=pltpu.CompilerParams(vmem_limit_bytes=16 << 20),
@@ -115,14 +113,12 @@
 
 
 def grad_kernel(counts, taps, swish, slope, gate, inputs, w_gate, w_up, *refs):
-    acts, downs, _, (terms_out, taps_out), grads_out, down_out, (terms,) = taken(refs, counts)
+    acts, (down, _, terms_out), grads_out, down_out, (terms,) = taken(refs, counts)
     c = pl.program_id(0)
-    for i, down in enumerate(downs):
-        for j in range(len(down_out) // len(downs)):
-
-            @pl.when(c == j)
-            def copy(ref=down_out[j * len(downs) + i], down=down):
-                ref[...] = down[...]
+
+    @pl.when(c == 0)
+    def copy():
+        split_rows(down_out, down)
 
     act_grad = jnp.concatenate([a[:, lanes_of(c)] for a in acts], 0).astype(jnp.float32)
     up_part = (act_grad * swish[...].astype(jnp.float32)).astype(jnp.bfloat16)
@@ -137,10 +133,11 @@
         jnp.sum(ahead * gate_float, axis=0, keepdims=True)
         for ahead in (ahead_two, ahead_one, conv_grad)
     ]
-    taps_out[:, lanes_of(c)] = jnp.concatenate(sums, 0).astype(jnp.bfloat16)
+    sums = jnp.concatenate(sums + [jnp.zeros((8 - TAPS, LANES), jnp.float32)], 0)
     parts = jnp.concatenate([gate_part, up_part], 1)
     grads = product(inputs[...], parts, ((1,), (0,))).astype(jnp.bfloat16)
-    split_rows(grads_out, jnp.concatenate([grads[:, :LANES], grads[:, LANES:]], 0), lanes_of(c))
+    columns = [grads[:, :LANES], grads[:, LANES:], sums.astype(jnp.bfloat16)]
+    split_rows(grads_out, jnp.concatenate(columns, 0), lanes_of(c))
     weights = jnp.concatenate([w_gate[...], w_up[...]], 1)
     term = product(weights, parts, ((1,), (1,)))
 
@@ -157,18 +154,15 @@
         terms_out[...] = terms[...].astype(jnp.bfloat16)
 
 
-def grad_cells(conv_taps, swish, slope, gate_saved, inputs, w_gate, w_up, acts, downs, extra):
+def grad_cells(conv_taps, swish, slope, gate_saved, inputs, w_gate, w_up, acts, down, extra):
     tokens, hidden = swish.shape
     block = inputs.shape[0]
     columns = pl.BlockSpec((tokens, LANES), lambda c: (0, c))
     weights = pl.BlockSpec((block, LANES), lambda c: (0, c))
-    grads = slabs(2 * block, ROWS, hidden)
+    grads = slabs(2 * block + 8, ROWS, hidden)
     kept = slabs(hidden, DOWN_ROWS, block)
-    out = [
-        pltpu.HBM((block, tokens), jnp.bfloat16),
-        pltpu.VMEM((TAPS, hidden), jnp.bfloat16),
-    ] + grads + kept
-    counts = [len(acts), len(downs), 1, 2, len(grads), len(kept)]
+    out = [pltpu.HBM((block, tokens), jnp.bfloat16)] + grads + kept
+    counts = [len(acts), 3, len(grads), len(kept)]
     return pl.pallas_call(
         lambda *refs: grad_kernel(counts, *refs),
         out_shape=out,
@@ -176,51 +170,55 @@
         in_specs=[pl.BlockSpec((TAPS, LANES), lambda c: (0, c)), columns, columns, columns]
         + [whole(inputs), weights, weights]
         + [whole(a) for a in acts]
-        + [pl.BlockSpec((DOWN_ROWS, block), lambda c: (c, 0))] * len(downs)
-        + [pl.BlockSpec(memory_space=pl.ANY)],
+        + [whole(down), pl.BlockSpec(memory_space=pl.ANY)],
         out_specs=[whole(o) for o in out],
         scratch_shapes=[pltpu.VMEM((block, tokens), jnp.float32)],
         compiler_params=pltpu.CompilerParams(vmem_limit_bytes=24 << 20),
         name="grad_cells",
-    )(conv_taps, swish, slope, gate_saved, inputs, w_gate, w_up, *acts, *downs, extra)
+    )(conv_taps, swish, slope, gate_saved, inputs, w_gate, w_up, *acts, down, extra)
 
 
 def widen_kernel(counts, *refs):
-    pairs, downs, (taps, _), (gate_out, up_out, down_out, taps_out) = taken(refs, counts)
+    pairs, downs, (terms, _, input_out, gate_out, up_out, down_out, taps_out), _ = taken(refs, counts)
     block = gate_out.shape[0]
+    bounds = ((gate_out, 0, block), (up_out, block, 2 * block), (taps_out, 2 * block, 2 * block + TAPS))
     start = 0
     for ref in pairs:
-        rows = ref.shape[0]
         values = ref[...].astype(jnp.float32)
-        cut = min(max(block - start, 0), rows)
-        if cut > 0:
-            gate_out[start : start + cut, :] = values[:cut]
-        if cut < rows:
-            up_out[start + cut - block : start + rows - block, :] = values[cut:]
-        start += rows
-    for i, ref in enumerate(downs):
-        down_out[i * DOWN_ROWS : (i + 1) * DOWN_ROWS, :] = ref[...].astype(jnp.float32)
-    taps_out[...] = taps[...].astype(jnp.float32)
-
-
-def widened(pairs, downs, taps, extra):
-    hidden = taps.shape[1]
+        for out, low, high in bounds:
+            first, last = max(low, start), min(high, start + ref.shape[0])
+            if first < last:
+                out[first - low : last - low, :] = values[first - start : last - start]
+        start += ref.shape[0]
+    start = 0
+    for ref in downs:
+        down_out[start : start + ref.shape[0], :] = ref[...].astype(jnp.float32)
+        start += ref.shape[0]
+    total = terms[0].astype(jnp.float32)
+    for i in range(1, terms.shape[0]):
+        total = total + terms[i].astype(jnp.float32)
+    input_out[...] = total.astype(jnp.bfloat16)
+
+
+def widened(pairs, downs, terms, extra):
+    hidden = pairs[0].shape[1]
     block = downs[0].shape[1]
     grads = jax.ShapeDtypeStruct((block, hidden), jnp.float32)
-    counts = [len(pairs), len(downs), 2]
+    counts = [len(pairs), len(downs), 7]
     return pl.pallas_call(
         lambda *refs: widen_kernel(counts, *refs),
         out_shape=[
+            jax.ShapeDtypeStruct(terms.shape[1:], jnp.bfloat16),
             grads,
             grads,
             jax.ShapeDtypeStruct((hidden, block), jnp.float32),
             jax.ShapeDtypeStruct((TAPS, hidden), jnp.float32),
         ],
-        in_specs=[pl.BlockSpec(memory_space=pltpu.VMEM)] * (sum(counts) - 1)
+        in_specs=[pl.BlockSpec(memory_space=pltpu.VMEM)] * (len(pairs) + len(downs) + 1)
         + [pl.BlockSpec(memory_space=pl.ANY)],
         compiler_params=pltpu.CompilerParams(vmem_limit_bytes=16 << 20),
         name="widened",
-    )(*pairs, *downs, taps, extra)
+    )(*pairs, *downs, terms, extra)
 
 
 def local(layer_input, gate_saved, up_saved, out_grad, conv_taps, w_gate, w_up, w_down):
@@ -232,30 +230,27 @@
     tokens = out_grad.shape[0]
     block = w_gate.shape[0]
     place = lax.axis_index("fs").astype(jnp.int32).reshape(1)
-    run = LANES // DOWN_ROWS
-    swish, slope, copies, one, *rest = conv_cells(
+    swish, slope, copies, one, down, *acts = conv_cells(
         place, gate_saved, up_saved, conv_taps, out_grad, w_down, layer_input, tp
     )
-    downs, acts = rest[:run], rest[run:]
     inputs = lax.all_to_all(copies, "tp", 0, 0, tiled=True).reshape(block, tokens)
     *acts, extra = lax.psum([*acts, one], "fs")
     acts = [pltpu.with_memory_space_constraint(a, pltpu.VMEM) for a in acts]
     inputs = pltpu.with_memory_space_constraint(inputs, pltpu.VMEM)
-    swish, slope, *downs = [
-        pltpu.with_memory_space_constraint(a, pltpu.HBM) for a in (swish, slope, *downs)
+    swish, slope, down = [
+        pltpu.with_memory_space_constraint(a, pltpu.HBM) for a in (swish, slope, down)
     ]
-    terms, taps, *grads = grad_cells(
-        conv_taps, swish, slope, gate_saved, inputs, w_gate, w_up, acts, downs, extra
+    terms, *grads = grad_cells(
+        conv_taps, swish, slope, gate_saved, inputs, w_gate, w_up, acts, down, extra
     )
     terms = lax.all_to_all(terms.reshape(tp, block // tp, tokens), "tp", 0, 0, tiled=True)
-    input_grad = jnp.sum(terms.astype(jnp.float32), axis=0).astype(jnp.bfloat16).T
-    *grads, taps, extra = lax.psum([*grads, taps, one], "rep")
-    *grads, taps = [pltpu.with_memory_space_constraint(a, pltpu.VMEM) for a in (*grads, taps)]
-    count = -(-2 * block // ROWS)
-    gate_grad, up_grad, down_grad, taps_grad = widened(
-        grads[:count], grads[count:], taps, extra
-    )
-    return (input_grad, gate_grad, up_grad, down_grad, taps_grad)
+    *grads, extra = lax.psum([*grads, one], "rep")
+    grads = [pltpu.with_memory_space_constraint(a, pltpu.VMEM) for a in grads]
+    count = len(slabs(2 * block + 8, ROWS, 1))
+    input_grad, gate_grad, up_grad, down_grad, taps_grad = widened(
+        grads[:count], grads[count:], terms, extra
+    )
+    return (input_grad.T, gate_grad, up_grad, down_grad, taps_grad)
 
 
 def solution(mesh):

time: 150 us -> 149 us (level)
  transfers between devices with their start and end apart: 2 -> 2, of which waited for: 0 -> 0; matrix products, arithmetic and copies ran while one was open for 0% -> 0% of each run, Pallas kernels for 1% -> 0%
where the time goes in v4:
time: 149 us
  blocking collectives  112 us (75%)
  starting transfers between devices  21.3 us (14%)
  Pallas kernels  15.2 us (10%)
    psum x1, blocking collectives, local(): *grads, extra = lax.psum([*grads, one], 'rep')  74.6 us
    psum x1, blocking collectives, local(): *acts, extra = lax.psum([*acts, one], 'fs')  37 us
    all_to_all x1, starting transfers between devices, local(): lax.all_to_all(copies, 'tp', 0, 0, tiled=True).reshape(block, tokens)  16.5 us
    pallas_call x1, Pallas kernels, grad_cells(): pl.pallas_call(lambda *refs: grad_kernel(counts, *refs), out_shape=out, g...  7.19 us
    pallas_call x1, Pallas kernels, conv_cells(): pl.pallas_call(conv_kernel, out_shape=[cells, cells, copies, one, down] +...  6.04 us
    all_to_all x1, starting transfers between devices, local(): lax.all_to_all(terms.reshape(tp, block // tp, tokens), 'tp', 0, 0, tiled=...  4.8 us
  transfers between devices with their start and end apart: 2, of which 0 were waited for; matrix products, arithmetic and copies ran while one was open for 0% of the time, Pallas kernels for 0%

profile of v4, /device:TPU:6, one launch (start us, length us, event | category | flops | bytes accessed | tf_op | source)
XLA Modules:
  0.0 148.7 jit_solution(9952967662915093406)
XLA Ops:
  0.6 6.0 %conv_cells.1 = (bf16[768,640]{1,0:T(8,128)(2,1)}, bf16[768,640]{1,0:T(8,128)(2,1)}, bf16[8,32,768]{2,1,0:T(8,128)(2,1)}, bf16[1,1]{1,0:T(2,128)(2,1)}, bf16[640...) custom-call(s32[1]{0:T(128)} %bitcast.place, ...), custom_call_target="tpu_custom_call" | custom-call | tf_op jit(solution)/shard_map/conv_cells/pallas_call | solution.py:84
  6.7 16.5 %all-to-all-start = ((bf16[8,32,768]{2,1,0:T(8,128)(2,1)}), bf16[8,32,768]{2,1,0:T(8,128)(2,1)S(1)}, u32[]{:S(2)}, u32[]{:S(2)}) async-start(bf16[8,32,768]{2,1,0:T(8,128)(2,1)} %get-tuple-element.51), calls=%async_computation | async-start | bytes 786432 | tf_op jit(solution)/shard_map/all_to_all | solution.py:236
  23.2 37.0 %all-reduce.4 = (bf16[48,640]{1,0:T(8,128)(2,1)S(1)}, bf16[48,640]{1,0:T(8,128)(2,1)S(1)}, bf16[48,640]{1,0:T(8,128)(2,1)S(1)}, bf16[48,640]{1,0:T(8,128)(2,1)S(...) all-reduce(bf16[48,640]{1,0:T(8,128)(2,1)S(1)} %get-tuple-element.5, ...), channel_id=1, replica_groups=mesh['rep'=16,'fs'=8,'tp'=8] {'fs'}, use_global_device_ids=true, to_apply=%region_0.0 | all-reduce | flops 491521 | bytes 1966084 | tf_op jit(solution)/shard_map/psum | solution.py:237
  60.1 0.0 all-to-all-done
  60.1 7.2 %grad_cells.1 = (bf16[256,768]{1,0:T(8,128)(2,1)}, bf16[48,640]{1,0:T(8,128)(2,1)S(1)}, bf16[48,640]{1,0:T(8,128)(2,1)S(1)}, bf16[48,640]{1,0:T(8,128)(2,1)S(1)}...) custom-call(bf16[3,640]{1,0:T(4,128)(2,1)} %refs_0_.1, ...), custom_call_target="tpu_custom_call" | custom-call | tf_op jit(solution)/shard_map/grad_cells/pallas_call | solution.py:166
  67.3 4.8 %all-to-all-start.1 = ((bf16[8,32,768]{2,1,0:T(8,128)(2,1)}), bf16[8,32,768]{2,1,0:T(8,128)(2,1)S(1)}, u32[]{:S(2)}, u32[]{:S(2)}) async-start(bf16[8,32,768]{2,1,0:T(8,128)(2,1)} %bitcast.6), calls=%async_computation.1 | async-start | bytes 786432 | tf_op jit(solution)/shard_map/all_to_all | solution.py:246
  72.1 74.6 %all-reduce.5 = (bf16[48,640]{1,0:T(8,128)(2,1)S(1)}, bf16[48,640]{1,0:T(8,128)(2,1)S(1)}, bf16[48,640]{1,0:T(8,128)(2,1)S(1)}, bf16[48,640]{1,0:T(8,128)(2,1)S(...) all-reduce(bf16[48,640]{1,0:T(8,128)(2,1)S(1)} %get-tuple-element.7, ...), channel_id=1, replica_groups=mesh['rep'=16,'fs'=8,'tp'=8] {'rep'}, use_global_device_ids=true, to_apply=%region_17.0 | all-reduce | flops 496641 | bytes 1986564 | tf_op jit(solution)/shard_map/psum | solution.py:247
  146.7 0.0 all-to-all-done.1.refs_17_
  146.7 2.0 %widened.1 = (bf16[32,768]{1,0:T(8,128)(2,1)}, f32[256,640]{1,0:T(8,128)}, f32[256,640]{1,0:T(8,128)}, f32[640,256]{1,0:T(8,128)}, f32[3,640]{1,0:T(4,128)}) custom-call(bf16[48,640]{1,0:T(8,128)(2,1)S(1)} %get-tuple-element.93.refs_0_, bf16[48,640]{1,0:T(8,128)(2,1)S(1)} %get-tuple-element.94.refs_1_, bf16[48,640]{1,0:T(8,128)(2,1)S(1)} %get-tuple-element.95.refs_2_, ...), custom_call_target="tpu_custom_call" | custom-call | tf_op jit(solution)/shard_map/widened/pallas_call | solution.py:208
Async XLA Ops:
  6.7 53.5 %all-to-all-start = ((bf16[8,32,768]{2,1,0:T(8,128)(2,1)}), bf16[8,32,768]{2,1,0:T(8,128)(2,1)S(1)}, u32[]{:S(2)}, u32[]{:S(2)}) async-start(bf16[8,32,768]{2,1,0:T(8,128)(2,1)} %get-tuple-element.51), calls=%async_computation | async-start | bytes 786432 | tf_op jit(solution)/shard_map/all_to_all | solution.py:236
  67.3 79.4 %all-to-all-start.1 = ((bf16[8,32,768]{2,1,0:T(8,128)(2,1)}), bf16[8,32,768]{2,1,0:T(8,128)(2,1)S(1)}, u32[]{:S(2)}, u32[]{:S(2)}) async-start(bf16[8,32,768]{2,1,0:T(8,128)(2,1)} %bitcast.6), calls=%async_computation.1 | async-start | bytes 786432 | tf_op jit(solution)/shard_map/all_to_all | solution.py:246

commit v5 on v4

--- a/solution.py
+++ b/solution.py
@@ -25,7 +25,7 @@
 
 
 def lanes_of(c):
-    return pl.ds(pl.multiple_of(c * LANES, LANES), LANES)
+    return slice(c * LANES, (c + 1) * LANES)
 
 
 def split_rows(out, values, lanes=slice(None)):
@@ -47,36 +47,33 @@
 
 def conv_kernel(place, gate, up, taps, grad, down, inputs, *refs):
     swish_out, slope_out, copies_out, one_out, down_out, *act_out = refs
-
-    @pl.when(pl.program_id(0) == 0)
-    def first():
-        one_out[...] = taps[0:1, 0:1]
-        for i in range(copies_out.shape[0]):
-            copies_out[i] = inputs[...]
-
-    share = product(grad[...], down[...], ((1,), (1,))).astype(jnp.bfloat16)
-    split_rows(act_out, share, lanes_of(pl.program_id(0)))
-    gate_float = gate[...].astype(jnp.float32)
-    up_float = up[...].astype(jnp.float32)
-    taps_float = taps[...].astype(jnp.float32)
-    conv_out = (
-        taps_float[0:1] * moved(gate_float, 2)
-        + taps_float[1:2] * moved(gate_float, 1)
-        + taps_float[2:3] * gate_float
-    )
-    sig = 0.5 * jnp.tanh(0.5 * conv_out) + 0.5
-    swish = conv_out * sig
-    swish_out[...] = swish.astype(jnp.bfloat16)
-    slope_out[...] = (up_float * (sig + swish * (1.0 - sig))).astype(jnp.bfloat16)
-    activation = (swish * up_float).astype(jnp.bfloat16)
-    down_out[...] = product(activation, grad[...], ((0,), (0,))).astype(jnp.bfloat16)
+    one_out[...] = taps[0:1, 0:1]
+    for i in range(copies_out.shape[0]):
+        copies_out[i] = inputs[...]
+    for c in range(gate.shape[1] // LANES):
+        lanes = lanes_of(c)
+        share = product(grad[...], down[lanes, :], ((1,), (1,))).astype(jnp.bfloat16)
+        split_rows(act_out, share, lanes)
+        gate_float = gate[:, lanes].astype(jnp.float32)
+        up_float = up[:, lanes].astype(jnp.float32)
+        taps_float = taps[:, lanes].astype(jnp.float32)
+        conv_out = (
+            taps_float[0:1] * moved(gate_float, 2)
+            + taps_float[1:2] * moved(gate_float, 1)
+            + taps_float[2:3] * gate_float
+        )
+        sig = 0.5 * jnp.tanh(0.5 * conv_out) + 0.5
+        swish = conv_out * sig
+        swish_out[:, lanes] = swish.astype(jnp.bfloat16)
+        slope_out[:, lanes] = (up_float * (sig + swish * (1.0 - sig))).astype(jnp.bfloat16)
+        activation = (swish * up_float).astype(jnp.bfloat16)
+        down_out[lanes, :] = product(activation, grad[...], ((0,), (0,))).astype(jnp.bfloat16)
 
 
 def conv_cells(place, gate_saved, up_saved, conv_taps, out_grad, w_down, inputs, copies):
     tokens, hidden = gate_saved.shape
     block = w_down.shape[1]
     acts = slabs(tokens, ROWS, hidden)
-    columns = pl.BlockSpec((tokens, LANES), lambda c, s: (0, c))
     cells = pltpu.HBM((tokens, hidden), jnp.bfloat16)
     copies = pltpu.HBM((copies, *inputs.shape), inputs.dtype)
     one = jax.ShapeDtypeStruct((1, 1), jnp.bfloat16)
@@ -86,20 +83,19 @@
         out_shape=[cells, cells, copies, one, down] + acts,
         grid_spec=pltpu.PrefetchScalarGridSpec(
             num_scalar_prefetch=1,
-            grid=(hidden // LANES,),
+            grid=(1,),
             in_specs=[
-                columns,
-                columns,
-                pl.BlockSpec((TAPS, LANES), lambda c, s: (0, c)),
+                whole(gate_saved),
+                whole(up_saved),
+                whole(conv_taps),
                 pl.BlockSpec((tokens, block), lambda c, s: (0, s[0])),
-                pl.BlockSpec((LANES, block), lambda c, s: (c, 0)),
+                whole(w_down),
                 whole(inputs),
             ],
-            out_specs=[columns, columns, whole(copies), whole(one)]
-            + [pl.BlockSpec((LANES, block), lambda c, s: (c, 0))]
+            out_specs=[whole(a) for a in (cells, cells, copies, one, down)]
             + [whole(a) for a in acts],
         ),
-        compiler_params=pltpu.CompilerParams(vmem_limit_bytes=16 << 20),
+        compiler_params=pltpu.CompilerParams(vmem_limit_bytes=32 << 20),
         name="conv_cells",
     )(place, gate_saved, up_saved, conv_taps, out_grad, w_down, inputs)
 
@@ -114,51 +110,41 @@
 
 def grad_kernel(counts, taps, swish, slope, gate, inputs, w_gate, w_up, *refs):
     acts, (down, _, terms_out), grads_out, down_out, (terms,) = taken(refs, counts)
-    c = pl.program_id(0)
-
-    @pl.when(c == 0)
-    def copy():
-        split_rows(down_out, down)
-
-    act_grad = jnp.concatenate([a[:, lanes_of(c)] for a in acts], 0).astype(jnp.float32)
-    up_part = (act_grad * swish[...].astype(jnp.float32)).astype(jnp.bfloat16)
-    conv_grad = act_grad * slope[...].astype(jnp.float32)
-    taps_float = taps[...].astype(jnp.float32)
-    ahead_one, ahead_two = moved(conv_grad, -1), moved(conv_grad, -2)
-    gate_part = (
-        taps_float[0:1] * ahead_two + taps_float[1:2] * ahead_one + taps_float[2:3] * conv_grad
-    ).astype(jnp.bfloat16)
-    gate_float = gate[...].astype(jnp.float32)
-    sums = [
-        jnp.sum(ahead * gate_float, axis=0, keepdims=True)
-        for ahead in (ahead_two, ahead_one, conv_grad)
-    ]
-    sums = jnp.concatenate(sums + [jnp.zeros((8 - TAPS, LANES), jnp.float32)], 0)
-    parts = jnp.concatenate([gate_part, up_part], 1)
-    grads = product(inputs[...], parts, ((1,), (0,))).astype(jnp.bfloat16)
-    columns = [grads[:, :LANES], grads[:, LANES:], sums.astype(jnp.bfloat16)]
-    split_rows(grads_out, jnp.concatenate(columns, 0), lanes_of(c))
-    weights = jnp.concatenate([w_gate[...], w_up[...]], 1)
-    term = product(weights, parts, ((1,), (1,)))
-
-    @pl.when(c == 0)
-    def first():
-        terms[...] = term
-
-    @pl.when(c > 0)
-    def later():
-        terms[...] += term
-
-    @pl.when(c == pl.num_programs(0) - 1)
-    def last():
-        terms_out[...] = terms[...].astype(jnp.bfloat16)
+    split_rows(down_out, down)
+    count = swish.shape[1] // LANES
+    for c in range(count):
+        lanes = lanes_of(c)
+        act_grad = jnp.concatenate([a[:, lanes] for a in acts], 0).astype(jnp.float32)
+        up_part = (act_grad * swish[:, lanes].astype(jnp.float32)).astype(jnp.bfloat16)
+        conv_grad = act_grad * slope[:, lanes].astype(jnp.float32)
+        taps_float = taps[:, lanes].astype(jnp.float32)
+        ahead_one, ahead_two = moved(conv_grad, -1), moved(conv_grad, -2)
+        gate_part = (
+            taps_float[0:1] * ahead_two + taps_float[1:2] * ahead_one + taps_float[2:3] * conv_grad
+        ).astype(jnp.bfloat16)
+        gate_float = gate[:, lanes].astype(jnp.float32)
+        sums = [
+            jnp.sum(ahead * gate_float, axis=0, keepdims=True)
+            for ahead in (ahead_two, ahead_one, conv_grad)
+        ]
+        sums = jnp.concatenate(sums + [jnp.zeros((8 - TAPS, LANES), jnp.float32)], 0)
+        parts = jnp.concatenate([gate_part, up_part], 1)
+        grads = product(inputs[...], parts, ((1,), (0,))).astype(jnp.bfloat16)
+        columns = [grads[:, :LANES], grads[:, LANES:], sums.astype(jnp.bfloat16)]
+        split_rows(grads_out, jnp.concatenate(columns, 0), lanes)
+        weights = jnp.concatenate([w_gate[:, lanes], w_up[:, lanes]], 1)
+        term = product(weights, parts, ((1,), (1,)))
+        if c == 0:
+            terms[...] = term
+        elif c < count - 1:
+            terms[...] += term
+        else:
+            terms_out[...] = (terms[...] + term).astype(jnp.bfloat16)
 
 
 def grad_cells(conv_taps, swish, slope, gate_saved, inputs, w_gate, w_up, acts, down, extra):
     tokens, hidden = swish.shape
     block = inputs.shape[0]
-    columns = pl.BlockSpec((tokens, LANES), lambda c: (0, c))
-    weights = pl.BlockSpec((block, LANES), lambda c: (0, c))
     grads = slabs(2 * block + 8, ROWS, hidden)
     kept = slabs(hidden, DOWN_ROWS, block)
     out = [pltpu.HBM((block, tokens), jnp.bfloat16)] + grads + kept
@@ -166,14 +152,13 @@
     return pl.pallas_call(
         lambda *refs: grad_kernel(counts, *refs),
         out_shape=out,
-        grid=(hidden // LANES,),
-        in_specs=[pl.BlockSpec((TAPS, LANES), lambda c: (0, c)), columns, columns, columns]
-        + [whole(inputs), weights, weights]
+        grid=(1,),
+        in_specs=[whole(a) for a in (conv_taps, swish, slope, gate_saved, inputs, w_gate, w_up)]
         + [whole(a) for a in acts]
         + [whole(down), pl.BlockSpec(memory_space=pl.ANY)],
         out_specs=[whole(o) for o in out],
         scratch_shapes=[pltpu.VMEM((block, tokens), jnp.float32)],
-        compiler_params=pltpu.CompilerParams(vmem_limit_bytes=24 << 20),
+        compiler_params=pltpu.CompilerParams(vmem_limit_bytes=32 << 20),
         name="grad_cells",
     )(conv_taps, swish, slope, gate_saved, inputs, w_gate, w_up, *acts, down, extra)
 

time: 149 us -> 146 us (0.980)
  Pallas kernels: 15.2 us -> 12.6 us
    pallas_call x1, Pallas kernels: 7.19 us -> 5.53 us  [grad_cells(): pl.pallas_call(lambda *refs: grad_kernel(counts, *refs), out_shape=out, g...]
where the time goes in v5:
time: 146 us
  blocking collectives  111 us (76%)
  starting transfers between devices  21.3 us (15%)
  Pallas kernels  12.6 us (9%)
    psum x1, blocking collectives, local(): *grads, extra = lax.psum([*grads, one], 'rep')  74.2 us
    psum x1, blocking collectives, local(): *acts, extra = lax.psum([*acts, one], 'fs')  37 us
    all_to_all x1, starting transfers between devices, local(): lax.all_to_all(copies, 'tp', 0, 0, tiled=True).reshape(block, tokens)  16.5 us
    pallas_call x1, Pallas kernels, grad_cells(): pl.pallas_call(lambda *refs: grad_kernel(counts, *refs), out_shape=out, g...  5.53 us
    pallas_call x1, Pallas kernels, conv_cells(): pl.pallas_call(conv_kernel, out_shape=[cells, cells, copies, one, down] +...  5.08 us
    all_to_all x1, starting transfers between devices, local(): lax.all_to_all(terms.reshape(tp, block // tp, tokens), 'tp', 0, 0, tiled=...  4.8 us
  transfers between devices with their start and end apart: 2, of which 0 were waited for; matrix products, arithmetic and copies ran while one was open for 0% of the time, Pallas kernels for 0%

profile of v5, /device:TPU:6, one launch (start us, length us, event | category | flops | bytes accessed | tf_op | source)
XLA Modules:
  0.0 145.7 jit_solution(6243887200093450474)
XLA Ops:
  0.6 5.1 %conv_cells.1 = (bf16[768,640]{1,0:T(8,128)(2,1)}, bf16[768,640]{1,0:T(8,128)(2,1)}, bf16[8,32,768]{2,1,0:T(8,128)(2,1)}, bf16[1,1]{1,0:T(2,128)(2,1)}, bf16[640...) custom-call(s32[1]{0:T(128)} %bitcast.place, ...), custom_call_target="tpu_custom_call" | custom-call | tf_op jit(solution)/shard_map/conv_cells/pallas_call | solution.py:81
  5.7 16.5 %all-to-all-start = ((bf16[8,32,768]{2,1,0:T(8,128)(2,1)}), bf16[8,32,768]{2,1,0:T(8,128)(2,1)S(1)}, u32[]{:S(2)}, u32[]{:S(2)}) async-start(bf16[8,32,768]{2,1,0:T(8,128)(2,1)} %get-tuple-element.51), calls=%async_computation | async-start | bytes 786432 | tf_op jit(solution)/shard_map/all_to_all | solution.py:221
  22.2 37.0 %all-reduce.4 = (bf16[48,640]{1,0:T(8,128)(2,1)S(1)}, bf16[48,640]{1,0:T(8,128)(2,1)S(1)}, bf16[48,640]{1,0:T(8,128)(2,1)S(1)}, bf16[48,640]{1,0:T(8,128)(2,1)S(...) all-reduce(bf16[48,640]{1,0:T(8,128)(2,1)S(1)} %get-tuple-element.5, ...), channel_id=1, replica_groups=mesh['rep'=16,'fs'=8,'tp'=8] {'fs'}, use_global_device_ids=true, to_apply=%region_0.0 | all-reduce | flops 491521 | bytes 1966084 | tf_op jit(solution)/shard_map/psum | solution.py:222
  59.2 0.0 all-to-all-done
  59.2 5.5 %grad_cells.1 = (bf16[256,768]{1,0:T(8,128)(2,1)}, bf16[48,640]{1,0:T(8,128)(2,1)S(1)}, bf16[48,640]{1,0:T(8,128)(2,1)S(1)}, bf16[48,640]{1,0:T(8,128)(2,1)S(1)}...) custom-call(bf16[3,640]{1,0:T(4,128)(2,1)} %refs_0_.1, ...), custom_call_target="tpu_custom_call" | custom-call | tf_op jit(solution)/shard_map/grad_cells/pallas_call | solution.py:152
  64.7 4.8 %all-to-all-start.1 = ((bf16[8,32,768]{2,1,0:T(8,128)(2,1)}), bf16[8,32,768]{2,1,0:T(8,128)(2,1)S(1)}, u32[]{:S(2)}, u32[]{:S(2)}) async-start(bf16[8,32,768]{2,1,0:T(8,128)(2,1)} %bitcast.6), calls=%async_computation.1 | async-start | bytes 786432 | tf_op jit(solution)/shard_map/all_to_all | solution.py:231
  69.5 74.2 %all-reduce.5 = (bf16[48,640]{1,0:T(8,128)(2,1)S(1)}, bf16[48,640]{1,0:T(8,128)(2,1)S(1)}, bf16[48,640]{1,0:T(8,128)(2,1)S(1)}, bf16[48,640]{1,0:T(8,128)(2,1)S(...) all-reduce(bf16[48,640]{1,0:T(8,128)(2,1)S(1)} %get-tuple-element.7, ...), channel_id=1, replica_groups=mesh['rep'=16,'fs'=8,'tp'=8] {'rep'}, use_global_device_ids=true, to_apply=%region_17.0 | all-reduce | flops 496641 | bytes 1986564 | tf_op jit(solution)/shard_map/psum | solution.py:232
  143.7 0.0 all-to-all-done.1.refs_17_
  143.7 2.0 %widened.1 = (bf16[32,768]{1,0:T(8,128)(2,1)}, f32[256,640]{1,0:T(8,128)}, f32[256,640]{1,0:T(8,128)}, f32[640,256]{1,0:T(8,128)}, f32[3,640]{1,0:T(4,128)}) custom-call(bf16[48,640]{1,0:T(8,128)(2,1)S(1)} %get-tuple-element.93.refs_0_, bf16[48,640]{1,0:T(8,128)(2,1)S(1)} %get-tuple-element.94.refs_1_, bf16[48,640]{1,0:T(8,128)(2,1)S(1)} %get-tuple-element.95.refs_2_, ...), custom_call_target="tpu_custom_call" | custom-call | tf_op jit(solution)/shard_map/widened/pallas_call | solution.py:193
Async XLA Ops:
  5.7 53.5 %all-to-all-start = ((bf16[8,32,768]{2,1,0:T(8,128)(2,1)}), bf16[8,32,768]{2,1,0:T(8,128)(2,1)S(1)}, u32[]{:S(2)}, u32[]{:S(2)}) async-start(bf16[8,32,768]{2,1,0:T(8,128)(2,1)} %get-tuple-element.51), calls=%async_computation | async-start | bytes 786432 | tf_op jit(solution)/shard_map/all_to_all | solution.py:221
  64.7 79.0 %all-to-all-start.1 = ((bf16[8,32,768]{2,1,0:T(8,128)(2,1)}), bf16[8,32,768]{2,1,0:T(8,128)(2,1)S(1)}, u32[]{:S(2)}, u32[]{:S(2)}) async-start(bf16[8,32,768]{2,1,0:T(8,128)(2,1)} %bitcast.6), calls=%async_computation.1 | async-start | bytes 786432 | tf_op jit(solution)/shard_map/all_to_all | solution.py:231

commit v6 on v5

--- a/solution.py
+++ b/solution.py
@@ -109,10 +109,10 @@
 
 
 def grad_kernel(counts, taps, swish, slope, gate, inputs, w_gate, w_up, *refs):
-    acts, (down, _, terms_out), grads_out, down_out, (terms,) = taken(refs, counts)
+    acts, (down, _, terms_out), grads_out, down_out, _ = taken(refs, counts)
     split_rows(down_out, down)
-    count = swish.shape[1] // LANES
-    for c in range(count):
+    gates, ups = [], []
+    for c in range(swish.shape[1] // LANES):
         lanes = lanes_of(c)
         act_grad = jnp.concatenate([a[:, lanes] for a in acts], 0).astype(jnp.float32)
         up_part = (act_grad * swish[:, lanes].astype(jnp.float32)).astype(jnp.bfloat16)
@@ -132,14 +132,11 @@
         grads = product(inputs[...], parts, ((1,), (0,))).astype(jnp.bfloat16)
         columns = [grads[:, :LANES], grads[:, LANES:], sums.astype(jnp.bfloat16)]
         split_rows(grads_out, jnp.concatenate(columns, 0), lanes)
-        weights = jnp.concatenate([w_gate[:, lanes], w_up[:, lanes]], 1)
-        term = product(weights, parts, ((1,), (1,)))
-        if c == 0:
-            terms[...] = term
-        elif c < count - 1:
-            terms[...] += term
-        else:
-            terms_out[...] = (terms[...] + term).astype(jnp.bfloat16)
+        gates.append(gate_part)
+        ups.append(up_part)
+    weights = jnp.concatenate([w_gate[...], w_up[...]], 1)
+    term = product(weights, jnp.concatenate(gates + ups, 1), ((1,), (1,)))
+    terms_out[...] = term.astype(jnp.bfloat16)
 
 
 def grad_cells(conv_taps, swish, slope, gate_saved, inputs, w_gate, w_up, acts, down, extra):
@@ -157,7 +154,6 @@
         + [whole(a) for a in acts]
         + [whole(down), pl.BlockSpec(memory_space=pl.ANY)],
         out_specs=[whole(o) for o in out],
-        scratch_shapes=[pltpu.VMEM((block, tokens), jnp.float32)],
         compiler_params=pltpu.CompilerParams(vmem_limit_bytes=32 << 20),
         name="grad_cells",
     )(conv_taps, swish, slope, gate_saved, inputs, w_gate, w_up, *acts, down, extra)

time: 146 us -> 147 us (level)
  no operation moved by 1% of the time
where the time goes in v6:
time: 147 us; the launch traced here: 146 us
  blocking collectives  111 us (76%)
  starting transfers between devices  21.3 us (14%)
  Pallas kernels  12.8 us (9%)
    psum x1, blocking collectives, local(): *grads, extra = lax.psum([*grads, one], 'rep')  74.2 us
    psum x1, blocking collectives, local(): *acts, extra = lax.psum([*acts, one], 'fs')  37 us
    all_to_all x1, starting transfers between devices, local(): lax.all_to_all(copies, 'tp', 0, 0, tiled=True).reshape(block, tokens)  16.5 us
    pallas_call x1, Pallas kernels, grad_cells(): pl.pallas_call(lambda *refs: grad_kernel(counts, *refs), out_shape=out, g...  5.73 us
    pallas_call x1, Pallas kernels, conv_cells(): pl.pallas_call(conv_kernel, out_shape=[cells, cells, copies, one, down] +...  5.08 us
    all_to_all x1, starting transfers between devices, local(): lax.all_to_all(terms.reshape(tp, block // tp, tokens), 'tp', 0, 0, tiled=...  4.79 us
  transfers between devices with their start and end apart: 2, of which 0 were waited for; matrix products, arithmetic and copies ran while one was open for 0% of the time, Pallas kernels for 0%

profile of v6, /device:TPU:6, one launch (start us, length us, event | category | flops | bytes accessed | tf_op | source)
XLA Modules:
  0.0 145.9 jit_solution(8383016018377942596)
XLA Ops:
  0.6 5.1 %conv_cells.1 = (bf16[768,640]{1,0:T(8,128)(2,1)}, bf16[768,640]{1,0:T(8,128)(2,1)}, bf16[8,32,768]{2,1,0:T(8,128)(2,1)}, bf16[1,1]{1,0:T(2,128)(2,1)}, bf16[640...) custom-call(s32[1]{0:T(128)} %bitcast.place, ...), custom_call_target="tpu_custom_call" | custom-call | tf_op jit(solution)/shard_map/conv_cells/pallas_call | solution.py:81
  5.7 16.5 %all-to-all-start = ((bf16[8,32,768]{2,1,0:T(8,128)(2,1)}), bf16[8,32,768]{2,1,0:T(8,128)(2,1)S(1)}, u32[]{:S(2)}, u32[]{:S(2)}) async-start(bf16[8,32,768]{2,1,0:T(8,128)(2,1)} %get-tuple-element.51), calls=%async_computation | async-start | bytes 786432 | tf_op jit(solution)/shard_map/all_to_all | solution.py:217
  22.2 37.0 %all-reduce.4 = (bf16[48,640]{1,0:T(8,128)(2,1)S(1)}, bf16[48,640]{1,0:T(8,128)(2,1)S(1)}, bf16[48,640]{1,0:T(8,128)(2,1)S(1)}, bf16[48,640]{1,0:T(8,128)(2,1)S(...) all-reduce(bf16[48,640]{1,0:T(8,128)(2,1)S(1)} %get-tuple-element.5, ...), channel_id=1, replica_groups=mesh['rep'=16,'fs'=8,'tp'=8] {'fs'}, use_global_device_ids=true, to_apply=%region_0.0 | all-reduce | flops 491521 | bytes 1966084 | tf_op jit(solution)/shard_map/psum | solution.py:218
  59.2 0.0 all-to-all-done
  59.2 5.7 %grad_cells.1 = (bf16[256,768]{1,0:T(8,128)(2,1)}, bf16[48,640]{1,0:T(8,128)(2,1)S(1)}, bf16[48,640]{1,0:T(8,128)(2,1)S(1)}, bf16[48,640]{1,0:T(8,128)(2,1)S(1)}...) custom-call(bf16[3,640]{1,0:T(4,128)(2,1)} %refs_0_.1, ...), custom_call_target="tpu_custom_call" | custom-call | tf_op jit(solution)/shard_map/grad_cells/pallas_call | solution.py:149
  64.9 4.8 %all-to-all-start.1 = ((bf16[8,32,768]{2,1,0:T(8,128)(2,1)}), bf16[8,32,768]{2,1,0:T(8,128)(2,1)S(1)}, u32[]{:S(2)}, u32[]{:S(2)}) async-start(bf16[8,32,768]{2,1,0:T(8,128)(2,1)} %bitcast.6), calls=%async_computation.1 | async-start | bytes 786432 | tf_op jit(solution)/shard_map/all_to_all | solution.py:227
  69.7 74.2 %all-reduce.5 = (bf16[48,640]{1,0:T(8,128)(2,1)S(1)}, bf16[48,640]{1,0:T(8,128)(2,1)S(1)}, bf16[48,640]{1,0:T(8,128)(2,1)S(1)}, bf16[48,640]{1,0:T(8,128)(2,1)S(...) all-reduce(bf16[48,640]{1,0:T(8,128)(2,1)S(1)} %get-tuple-element.7, ...), channel_id=1, replica_groups=mesh['rep'=16,'fs'=8,'tp'=8] {'rep'}, use_global_device_ids=true, to_apply=%region_17.0 | all-reduce | flops 496641 | bytes 1986564 | tf_op jit(solution)/shard_map/psum | solution.py:228
  143.9 0.0 all-to-all-done.1.refs_17_
  143.9 2.0 %widened.1 = (bf16[32,768]{1,0:T(8,128)(2,1)}, f32[256,640]{1,0:T(8,128)}, f32[256,640]{1,0:T(8,128)}, f32[640,256]{1,0:T(8,128)}, f32[3,640]{1,0:T(4,128)}) custom-call(bf16[48,640]{1,0:T(8,128)(2,1)S(1)} %get-tuple-element.93.refs_0_, bf16[48,640]{1,0:T(8,128)(2,1)S(1)} %get-tuple-element.94.refs_1_, bf16[48,640]{1,0:T(8,128)(2,1)S(1)} %get-tuple-element.95.refs_2_, ...), custom_call_target="tpu_custom_call" | custom-call | tf_op jit(solution)/shard_map/widened/pallas_call | solution.py:189
Async XLA Ops:
  5.7 53.5 %all-to-all-start = ((bf16[8,32,768]{2,1,0:T(8,128)(2,1)}), bf16[8,32,768]{2,1,0:T(8,128)(2,1)S(1)}, u32[]{:S(2)}, u32[]{:S(2)}) async-start(bf16[8,32,768]{2,1,0:T(8,128)(2,1)} %get-tuple-element.51), calls=%async_computation | async-start | bytes 786432 | tf_op jit(solution)/shard_map/all_to_all | solution.py:217
  64.9 79.0 %all-to-all-start.1 = ((bf16[8,32,768]{2,1,0:T(8,128)(2,1)}), bf16[8,32,768]{2,1,0:T(8,128)(2,1)S(1)}, u32[]{:S(2)}, u32[]{:S(2)}) async-start(bf16[8,32,768]{2,1,0:T(8,128)(2,1)} %bitcast.6), calls=%async_computation.1 | async-start | bytes 786432 | tf_op jit(solution)/shard_map/all_to_all | solution.py:227
